TPU v7x, 32 devices: a whole 2x2x4 slice. The times are simulated.
32 devices in a mesh: sp: 4 (over z), fs: 4 (over y, x), tp: 2 (over core).
Axes of the slice: x: 2, y: 2, z: 4, core: 2. Of those that a mesh axis runs over, the one named last changes fastest.
Arguments:
- activations: bfloat16 [4, 1024, 2048], P('fs', 'sp'), may hold values from -600 to 600
- norm_gain: float32 [2048], replicated, may hold values from 0.1 to 1.9
- w_conv_gate: bfloat16 [2048, 1024], P('sp', ('fs', 'tp')), may hold values from -0.125 to 0.125
- w_conv_mult: bfloat16 [2048, 1024], P('sp', ('fs', 'tp')), may hold values from -0.125 to 0.125
- w_conv_in: bfloat16 [2048, 1024], P('sp', ('fs', 'tp')), may hold values from -0.125 to 0.125
- conv_taps: float32 [3, 1024], replicated, may hold values from -3.5 to 3.5
- w_query: bfloat16 [2048, 1024], P('sp', ('fs', 'tp')), may hold values from -0.125 to 0.125
- w_key: bfloat16 [2048, 1024], P('sp', ('fs', 'tp')), may hold values from -0.125 to 0.125
- w_value: bfloat16 [2048, 1024], P('sp', ('fs', 'tp')), may hold values from -0.125 to 0.125
- w_input_gate: bfloat16 [2048, 8], replicated, may hold values from -0.125 to 0.125
- w_forget_gate: bfloat16 [2048, 8], replicated, may hold values from -0.125 to 0.125
- gate_bias: float32 [2, 8], replicated, may hold values from -1 to 120
- decay_shift: float32 [4, 1024, 8], P(None, 'sp'), may hold values from -2 to 0, as said below
- head_gain: float32 [1024], replicated, may hold values from 0.1 to 1.9
- w_out_conv: bfloat16 [1024, 2048], P(('fs', 'tp'), 'sp'), may hold values from -0.125 to 0.125
- w_out_mem: bfloat16 [1024, 2048], P(('fs', 'tp'), 'sp'), may hold values from -0.125 to 0.125
Outputs:
- output: bfloat16 [4, 1024, 2048], P('fs', ('sp', 'tp'))
Inputs may be any that keep to these rules, and one draw needn't show every extreme that they name: `decay_shift`: never positive.
All inputs are finite; a program needn't handle non-finite values.
Results may differ from a plain program's by a relative error of at most 0.015.
Values may be sent and summed in bfloat16 or wider, within the bound.
A program may use at most 64 MiB of HBM per device.

v0:
```python
import functools

import jax
import jax.numpy as jnp
from jax import lax
from jax.experimental import pallas as pl
from jax.experimental.pallas import tpu as pltpu
from jax.sharding import PartitionSpec as P

MEMORY_HEADS = 8
HEAD_DIM = 128
BLOCK = 64


EPSILON = 1e-06
FAR_BELOW = -1e30
HIGHEST_PRECISION = lax.Precision.HIGHEST


def later_kernel(ns, state_ref, stat_ref, states, stats, s_send, s_recv, t_send, t_recv):
    sp, fs, tp = (lax.axis_index("sp"), lax.axis_index("fs"), lax.axis_index("tp"))
    greet([(None, (lax.rem(sp + off, ns), fs, tp)) for off in range(1, ns)])

    def copies(off, source):
        to = (sp + off, fs, tp)
        return (
            pltpu.make_async_remote_copy(
                stat_ref, stats.at[source], t_send.at[off - 1], t_recv.at[off - 1],
                device_id=to, device_id_type=MESH,
            ),
            pltpu.make_async_remote_copy(
                state_ref, states.at[source], s_send.at[off - 1], s_recv.at[off - 1],
                device_id=to, device_id_type=MESH,
            ),
        )

    for off in range(1, ns):

        @pl.when(sp + off < ns)
        def _():
            for copy in copies(off, sp):
                copy.start()

    for off in range(1, ns):

        @pl.when(sp - off >= 0)
        def _():
            for copy in copies(off, sp - off):
                copy.wait_recv()

    for off in range(1, ns):

        @pl.when(sp + off < ns)
        def _():
            for copy in copies(off, sp):
                copy.wait_send()


def send_later(state, stats, ns):
    vmem = pl.BlockSpec(memory_space=pltpu.VMEM)
    return pl.pallas_call(
        functools.partial(later_kernel, ns),
        out_shape=(
            jax.ShapeDtypeStruct((ns,) + state.shape, state.dtype),
            jax.ShapeDtypeStruct((ns,) + stats.shape, stats.dtype),
        ),
        in_specs=[vmem, vmem],
        out_specs=(vmem, vmem),
        scratch_shapes=[pltpu.SemaphoreType.DMA((ns - 1,))] * 4,
        compiler_params=pltpu.CompilerParams(collective_id=2, has_side_effects=True),
    )(state, stats)


def prefix(value, axis, join, neutral):
    count, mine = (lax.axis_size(axis), lax.axis_index(axis))
    total, peak, state = value
    stats = jnp.stack([total, peak], axis=1)[..., None]
    stats = jnp.broadcast_to(stats, stats.shape[:2] + state.shape[-1:])
    stats = jnp.pad(stats, ((0, 0), (0, 6), (0, 0)))
    if count <= 8:
        states, stats = send_later(state.astype(jnp.bfloat16), stats, count)
        pieces = (stats[:, :, 0, 0], stats[:, :, 1, 0], states.astype(jnp.float32))
    else:
        packed = lax.all_gather(jnp.concatenate([state, stats], axis=1), axis)
        height = state.shape[1]
        pieces = (packed[:, :, height, 0], packed[:, :, height + 1, 0], packed[:, :, :height])
    subtotal = jax.tree.map(
        lambda part, zero: jnp.full_like(part, 0) + jnp.asarray(zero, part.dtype), value, neutral
    )

    def lap(position, subtotal):
        longer = join(subtotal, jax.tree.map(lambda part: part[position], pieces))
        return jax.tree.map(lambda new, old: jnp.where(position < mine, new, old), longer, subtotal)

    if count <= 8:
        for position in range(count - 1):
            subtotal = lap(position, subtotal)
        return subtotal
    return lax.fori_loop(0, count - 1, lap, subtotal)


def from_behind(array, axis, by):
    peers = lax.axis_size(axis)
    pairs = [(i, i + by) for i in range(peers) if 0 <= i + by < peers]
    return lax.ppermute(array, axis, pairs)


def combine_states(earlier, later):
    total_one, peak_one, state_one = earlier
    total_two, peak_two, state_two = later
    peak_new = jnp.maximum(total_two + peak_one, peak_two)
    scale_old = jnp.exp(total_two + peak_one - peak_new)
    scale_new = jnp.exp(peak_two - peak_new)
    return (
        total_one + total_two,
        peak_new,
        scale_old[..., None, None] * state_one + scale_new[..., None, None] * state_two,
    )


def head_rows(values, seq_count, heads_here):
    tokens = values.shape[1]
    split_heads = values.reshape(seq_count, tokens, heads_here, HEAD_DIM).transpose(0, 2, 1, 3)
    return split_heads.reshape(seq_count * heads_here, tokens, HEAD_DIM).astype(jnp.float32)


def gate_rows(values, seq_count, heads_here):
    tokens = values.shape[1]
    return values.transpose(0, 2, 1).reshape(seq_count * heads_here, tokens)


def memory_cell(query_rows, key_rows, value_rows, entry_gate, log_forget):
    members = query_rows.shape[0]
    tokens = query_rows.shape[1]
    head_width = query_rows.shape[2]
    nblocks = tokens // BLOCK
    block_shape = (members, nblocks, BLOCK, head_width)
    query_blocks = query_rows.reshape(block_shape)
    key_blocks = key_rows.reshape(block_shape) * head_width ** (-0.5)
    value_blocks = value_rows.reshape(block_shape)
    entry_blocks = entry_gate.reshape(members, nblocks, BLOCK)
    forget_sums = jnp.cumsum(log_forget.reshape(members, nblocks, BLOCK), axis=-1)
    block_total = forget_sums[..., -1]
    local_logs = block_total[..., None] - forget_sums + entry_blocks
    local_peak = jnp.max(local_logs, axis=-1)
    local_weights = jnp.exp(local_logs - local_peak[..., None])
    local_state = jnp.einsum(
        "bclv,bclk->bcvk",
        local_weights[..., None] * value_blocks,
        key_blocks,
        precision=HIGHEST_PRECISION,
    )

    def advance(running, block_item):
        return (combine_states(running, block_item), running)

    zero_sums = jnp.zeros((members,), jnp.float32)
    low_peaks = jnp.full((members,), FAR_BELOW, jnp.float32)
    zero_states = jnp.zeros((members, head_width, head_width), jnp.float32)
    block_items = (
        jnp.moveaxis(block_total, 1, 0),
        jnp.moveaxis(local_peak, 1, 0),
        jnp.moveaxis(local_state, 1, 0),
    )
    device_total, inner_states = lax.scan(advance, (zero_sums, low_peaks, zero_states), block_items)
    inner_states = tuple((jnp.moveaxis(tensor, 0, 1) for tensor in inner_states))
    total_sum, total_peak, total_state = device_total
    before = prefix(
        (total_sum, total_peak, total_state),
        "sp",
        combine_states,
        (zero_sums, low_peaks, zero_states),
    )
    opening = combine_states((zero_sums, zero_sums, zero_states), before)
    opening = tuple((tensor[:, None] for tensor in opening))
    _, prior_peak, prior_state = combine_states(opening, inner_states)
    positions = jnp.arange(BLOCK)
    causal_mask = positions[:, None] >= positions[None, :]
    pair_logs = jnp.where(
        causal_mask,
        forget_sums[..., :, None] - forget_sums[..., None, :] + entry_blocks[..., None, :],
        -jnp.inf,
    )
    carried_logs = forget_sums + prior_peak[..., None]
    row_peak = jnp.maximum(carried_logs, jnp.max(pair_logs, axis=-1))
    inner_weights = jnp.exp(pair_logs - row_peak[..., None])
    carried_weights = jnp.exp(carried_logs - row_peak)
    scores = inner_weights * jnp.einsum(
        "bcld,bcsd->bcls", query_blocks, key_blocks, precision=HIGHEST_PRECISION
    )
    numerator = carried_weights[..., None] * jnp.einsum(
        "bcvk,bclk->bclv", prior_state, query_blocks, precision=HIGHEST_PRECISION
    ) + jnp.einsum("bcls,bcsv->bclv", scores, value_blocks, precision=HIGHEST_PRECISION)
    return numerator.reshape(members, tokens, head_width)


MESH = pl.DeviceIdType.MESH


def greet(peers):
    barrier = pltpu.get_barrier_semaphore()
    total = 0
    for there, peer in peers:
        if there is None:
            pl.semaphore_signal(barrier, inc=1, device_id=peer, device_id_type=MESH)
            total = total + 1
        else:

            @pl.when(there)
            def _(peer=peer):
                pl.semaphore_signal(barrier, inc=1, device_id=peer, device_id_type=MESH)

            total = total + there.astype(jnp.int32)
    pl.semaphore_wait(barrier, total)


def gather_kernel(
    ns,
    nf,
    cuts,
    act_ref,
    gain_ref,
    w0_ref,
    w1_ref,
    w2_ref,
    w3_ref,
    w4_ref,
    w5_ref,
    wg_ref,
    wc_ref,
    wm_ref,
    proj_ref,
    gate_ref,
    wo_ref,
    acts,
    normed,
    wbuf,
    total,
    local_sem,
    a_send,
    a_recv,
    ad_send,
    ad_recv,
    w_send,
    w_recv,
    o_send,
    o_recv,
    p_send,
    p_recv,
    d_send,
    d_recv,
):
    sp, fs, tp = (lax.axis_index("sp"), lax.axis_index("fs"), lax.axis_index("tp"))
    g = fs * 2 + tp
    depth, cols = w0_ref.shape
    width = 6 * cols
    cut = width // cuts
    tokens, model = act_ref.shape
    half = tokens // 2
    ocols = wc_ref.shape[1]
    partner = (sp, fs, 1 - tp)
    has_up, has_down = (sp + 1 < ns, sp > 0)
    up, down = ((sp + 1, fs, tp), (sp - 1, fs, tp))

    own_rows = pl.ds(pl.multiple_of(sp * depth, depth), depth)
    locals_ = []
    for j, ref in enumerate((w0_ref, w1_ref, w2_ref, w3_ref, w4_ref, w5_ref)):
        locals_.append(
            pltpu.make_async_copy(
                ref, wbuf.at[own_rows, pl.ds(j * cols, cols)], local_sem.at[j]
            )
        )
    own_ocols = pl.ds(pl.multiple_of(sp * ocols, ocols), ocols)
    for m, ref in enumerate((wc_ref, wm_ref)):
        locals_.append(
            pltpu.make_async_copy(ref, wo_ref.at[g, m, :, own_ocols], local_sem.at[6 + m])
        )
    locals_.append(pltpu.make_async_copy(act_ref, acts.at[fs], local_sem.at[8]))
    for copy in locals_:
        copy.start()

    fs_peers = [(None, (sp, lax.rem(fs + off, nf), tp)) for off in range(1, nf)]
    greet(fs_peers + [(None, partner), (has_up, up), (has_down, down)])

    my_half = pl.ds(pl.multiple_of(tp * half, half), half)
    other_half = pl.ds(pl.multiple_of((1 - tp) * half, half), half)

    def act_copy(off, src_f):
        return pltpu.make_async_remote_copy(
            act_ref.at[my_half],
            acts.at[src_f, my_half],
            a_send.at[off - 1],
            a_recv.at[off - 1],
            device_id=(sp, lax.rem(fs + off, nf), tp),
            device_id_type=MESH,
        )

    def act_relay(off, src_f, rows):
        return pltpu.make_async_remote_copy(
            acts.at[src_f, rows],
            acts.at[src_f, rows],
            ad_send.at[off - 1],
            ad_recv.at[off - 1],
            device_id=partner,
            device_id_type=MESH,
        )

    def w_copy(side, d, owner, k):
        rows = pl.ds(pl.multiple_of(owner * depth, depth), depth)
        place = wbuf.at[rows, pl.ds(k * cut, cut)]
        return pltpu.make_async_remote_copy(
            place,
            place,
            w_send.at[side, d, k],
            w_recv.at[side, d, k],
            device_id=(up, down)[side],
            device_id_type=MESH,
        )

    def o_copy(side, d, owner):
        place = wo_ref.at[g, :, :, pl.ds(pl.multiple_of(owner * ocols, ocols), ocols)]
        return pltpu.make_async_remote_copy(
            place,
            place,
            o_send.at[side, d],
            o_recv.at[side, d],
            device_id=(up, down)[side],
            device_id_type=MESH,
        )

    def p_copy(owner, off, src_g):
        place = wo_ref.at[src_g, :, :, pl.ds(pl.multiple_of(owner * ocols, ocols), ocols)]
        return pltpu.make_async_remote_copy(
            place,
            place,
            p_send.at[owner, off - 1],
            p_recv.at[owner, off - 1],
            device_id=(sp, lax.rem(fs + off, nf), tp),
            device_id_type=MESH,
        )

    def d_copy(owner, off, src_g):
        place = wo_ref.at[src_g, :, :, pl.ds(pl.multiple_of(owner * ocols, ocols), ocols)]
        return pltpu.make_async_remote_copy(
            place,
            place,
            d_send.at[owner, off],
            d_recv.at[owner, off],
            device_id=partner,
            device_id_type=MESH,
        )

    def origin(off):
        return lax.rem(fs + nf - off, nf)

    def sends(side, d):
        if side == 0:
            return (sp - d >= 0) & has_up
        return (sp + d < ns) & has_down

    def owner_of(side, d):
        return sp - d if side == 0 else sp + d

    def arrives(side, d):
        return (sp - d >= 0) if side == 0 else (sp + d < ns)

    for off in range(1, nf):
        act_copy(off, fs).start()
    for copy in locals_:
        copy.wait()

    def send_z(side, d):
        @pl.when(sends(side, d))
        def _():
            o_copy(side, d, owner_of(side, d)).start()

    def send_w(side, d, k):
        @pl.when(sends(side, d))
        def _():
            w_copy(side, d, owner_of(side, d), k).start()

    for side in range(2):
        send_z(side, 0)
    for k in range(cuts):
        for side in range(2):
            send_w(side, 0, k)

    def spread(owner):
        for off in range(1, nf):
            p_copy(owner, off, g).start()
        d_copy(owner, 0, g).start()

    spread(sp)
    for off in range(1, nf):
        act_copy(off, origin(off)).wait_recv()
        act_relay(off, origin(off), my_half).start()

    def z_round(d):
        for side in range(2):

            @pl.when(arrives(side, d))
            def _():
                owner = owner_of(side, d)
                o_copy(side, d - 1, owner).wait_recv()
                if d < ns - 1:
                    send_z(side, d)
                spread(owner)

    for off in range(1, nf):
        act_relay(off, origin(off), other_half).wait_recv()

    step = 64

    def norm_rows(i, carry):
        f = i // (tokens // step)
        rows = pl.ds(pl.multiple_of(lax.rem(i, tokens // step) * step, step), step)
        x = acts[f, rows, :].astype(jnp.float32)
        scale = lax.rsqrt(jnp.mean(x * x, axis=-1, keepdims=True) + EPSILON)
        out = (x * scale * gain_ref[...]).astype(jnp.bfloat16)
        normed[pl.ds(pl.multiple_of(i * step, step), step), :] = out
        return carry

    lax.fori_loop(0, nf * tokens // step, norm_rows, 0)
    tile = tokens

    def multiply(owner, first):
        rows = pl.ds(pl.multiple_of(owner * depth, depth), depth)

        def body(i, carry):
            here = pl.ds(pl.multiple_of(i * tile, tile), tile)
            part = jnp.dot(
                normed[here, rows], wbuf[rows, :], preferred_element_type=jnp.float32
            )
            total[here, :] = part if first else total[here, :] + part
            return carry

        lax.fori_loop(0, nf, body, 0)

    z_round(1)
    multiply(sp, True)

    def gates(i, carry):
        here = pl.ds(pl.multiple_of(i * tile, tile), tile)
        gate_ref[here, :] = jnp.dot(
            normed[here, :], wg_ref[...], preferred_element_type=jnp.float32
        )
        return carry

    lax.fori_loop(0, nf, gates, 0)

    def collect(s, carry):
        for off in range(1, nf):
            src_g = origin(off) * 2 + tp
            p_copy(s, off, src_g).wait_recv()
            d_copy(s, off, src_g).start()
        return carry

    for d in range(1, ns):
        if d == ns - 1:
            lax.fori_loop(0, ns, collect, 0)
        for k in range(cuts):
            for side in range(2):

                @pl.when(arrives(side, d))
                def _():
                    w_copy(side, d - 1, owner_of(side, d), k).wait_recv()
                    if d < ns - 1:
                        send_w(side, d, k)

        for side in range(2):

            @pl.when(arrives(side, d))
            def _():
                multiply(owner_of(side, d), False)

        if d + 1 < ns:
            z_round(d + 1)

    def round_rows(i, carry):
        here = pl.ds(pl.multiple_of(i * tile, tile), tile)
        proj_ref[here, :] = total[here, :].astype(jnp.bfloat16)
        return carry

    lax.fori_loop(0, nf, round_rows, 0)

    def finish(s, carry):
        for off in range(nf):
            d_copy(s, off, origin(off) * 2 + 1 - tp).wait_recv()
            d_copy(s, off, origin(off) * 2 + tp).wait_send()
        for off in range(1, nf):
            p_copy(s, off, g).wait_send()
        return carry

    lax.fori_loop(0, ns, finish, 0)
    for off in range(1, nf):
        act_copy(off, fs).wait_send()
        act_relay(off, origin(off), my_half).wait_send()
    for side in range(2):
        for d in range(ns - 1):

            @pl.when(sends(side, d))
            def _():
                o_copy(side, d, owner_of(side, d)).wait_send()
                for k in range(cuts):
                    w_copy(side, d, owner_of(side, d), k).wait_send()


def gather_and_project(act, gain, weights, gate_weights, w_out_conv, w_out_mem):
    ns, nf = (lax.axis_size("sp"), lax.axis_size("fs"))
    tokens, model = act.shape
    depth, cols = weights[0].shape
    rows, ocols = w_out_conv.shape
    count = nf * tokens
    cuts = 2
    vmem = pl.BlockSpec(memory_space=pltpu.VMEM)
    hbm = pl.BlockSpec(memory_space=pltpu.MemorySpace.HBM)
    dma = pltpu.SemaphoreType.DMA
    return pl.pallas_call(
        functools.partial(gather_kernel, ns, nf, cuts),
        out_shape=(
            jax.ShapeDtypeStruct((count, 6 * cols), jnp.bfloat16),
            jax.ShapeDtypeStruct((count, gate_weights.shape[1]), jnp.float32),
            jax.ShapeDtypeStruct((nf * 2, 2, rows, ns * ocols), jnp.bfloat16),
        ),
        in_specs=[hbm, vmem] + [hbm] * 6 + [vmem, hbm, hbm],
        out_specs=(vmem, vmem, pl.BlockSpec(memory_space=pl.ANY)),
        scratch_shapes=[
            pltpu.VMEM((nf, tokens, model), jnp.bfloat16),
            pltpu.VMEM((count, model), jnp.bfloat16),
            pltpu.VMEM((ns * depth, 6 * cols), jnp.bfloat16),
            pltpu.VMEM((count, 6 * cols), jnp.float32),
            dma((9,)),
            dma((nf - 1,)),
            dma((nf - 1,)),
            dma((nf - 1,)),
            dma((nf - 1,)),
            dma((2, ns - 1, cuts)),
            dma((2, ns - 1, cuts)),
            dma((2, ns - 1)),
            dma((2, ns - 1)),
            dma((ns, nf - 1)),
            dma((ns, nf - 1)),
            dma((ns, nf)),
            dma((ns, nf)),
        ],
        compiler_params=pltpu.CompilerParams(
            collective_id=0, has_side_effects=True, vmem_limit_bytes=50 * 1024 * 1024
        ),
    )(act, gain, *weights, gate_weights, w_out_conv, w_out_mem)


def output_kernel(nf, mix_ref, wo_ref, out_ref, got, wbuf, acc, w_sem, send, recv, own_sem):
    sp, fs, tp = (lax.axis_index("sp"), lax.axis_index("fs"), lax.axis_index("tp"))
    group = nf * 2
    g = fs * 2 + tp
    loads = [
        pltpu.make_async_copy(wo_ref.at[pl.ds(i * 2, 2)], wbuf.at[pl.ds(i * 2, 2)], w_sem.at[i])
        for i in range(nf)
    ]
    for load in loads:
        load.start()
    own = pltpu.make_async_copy(mix_ref.at[g], got.at[g], own_sem)
    own.start()

    def peer(off):
        to = lax.rem(g + off, group)
        return (sp, to // 2, lax.rem(to, 2))

    greet([(None, peer(off)) for off in range(1, group)])

    def copy(off, to, source):
        return pltpu.make_async_remote_copy(
            mix_ref.at[to],
            got.at[source],
            send.at[off - 1],
            recv.at[off - 1],
            device_id=peer(off),
            device_id_type=MESH,
        )

    for off in range(1, group):
        copy(off, lax.rem(g + off, group), g).start()
    for load in loads:
        load.wait()
    own.wait()

    def add(source, first):
        part = jnp.dot(
            got[source, 0], wbuf[source, 0], preferred_element_type=jnp.float32
        ) + jnp.dot(got[source, 1], wbuf[source, 1], preferred_element_type=jnp.float32)
        acc[...] = part if first else acc[...] + part

    add(g, True)
    for off in range(1, group):
        source = lax.rem(g + group - off, group)
        copy(off, lax.rem(g + off, group), source).wait_recv()
        add(source, False)
    out_ref[...] = acc[...].astype(jnp.bfloat16)
    for off in range(1, group):
        copy(off, lax.rem(g + off, group), g).wait_send()


def exchange_and_merge(mix, wo):
    nf = lax.axis_size("fs")
    group, _, tokens, channels = mix.shape
    width = wo.shape[3]
    vmem = pl.BlockSpec(memory_space=pltpu.VMEM)
    dma = pltpu.SemaphoreType.DMA
    return pl.pallas_call(
        functools.partial(output_kernel, nf),
        out_shape=jax.ShapeDtypeStruct((tokens, width), jnp.bfloat16),
        in_specs=[vmem, pl.BlockSpec(memory_space=pltpu.MemorySpace.HBM)],
        out_specs=vmem,
        scratch_shapes=[
            pltpu.VMEM(mix.shape, jnp.bfloat16),
            pltpu.VMEM(wo.shape, jnp.bfloat16),
            pltpu.VMEM((tokens, width), jnp.float32),
            dma((nf,)),
            dma((group - 1,)),
            dma((group - 1,)),
            dma,
        ],
        compiler_params=pltpu.CompilerParams(
            collective_id=1, has_side_effects=True, vmem_limit_bytes=40 * 1024 * 1024
        ),
    )(mix, wo)


def shards(
    activations,
    norm_gain,
    w_conv_gate,
    w_conv_mult,
    w_conv_in,
    conv_taps,
    w_query,
    w_key,
    w_value,
    w_input_gate,
    w_forget_gate,
    gate_bias,
    decay_shift,
    head_gain,
    w_out_conv,
    w_out_mem,
):
    group_index = lax.axis_index(("fs", "tp"))
    heads_here = MEMORY_HEADS // (lax.axis_size("fs") * lax.axis_size("tp"))
    channels = w_conv_gate.shape[1]
    if lax.axis_size("sp") <= 8 and lax.axis_size("tp") == 2:
        seq_count, tokens = lax.axis_size("fs"), activations.shape[1]
        all_gates = jnp.concatenate([w_input_gate, w_forget_gate], axis=1)
        flat, gate_flat, full_out = gather_and_project(
            activations[0],
            norm_gain[None, :],
            (w_conv_gate, w_conv_mult, w_conv_in, w_query, w_key, w_value),
            all_gates,
            w_out_conv,
            w_out_mem,
        )
        conv_gate, conv_mult, conv_in, query, keys_proj, value = [
            flat[:, at * channels : (at + 1) * channels].reshape(seq_count, tokens, channels)
            for at in range(6)
        ]
        gate_values = jnp.concatenate(
            [
                lax.dynamic_slice_in_dim(
                    gate_flat, at + group_index * heads_here, heads_here, 1
                )
                for at in (0, MEMORY_HEADS)
            ],
            axis=1,
        ).reshape(seq_count, tokens, 2 * heads_here)
    else:
        full_out = None
        sequences = lax.all_gather(activations, "fs", axis=0, tiled=True)
        seq_count = sequences.shape[0]
        tokens = sequences.shape[1]
        model_width = sequences.shape[2]
        row_count = seq_count * tokens
        flat_rows = sequences.reshape(row_count, model_width).astype(jnp.float32)
        normed = (
            flat_rows
            * lax.rsqrt(jnp.mean(flat_rows * flat_rows, axis=-1, keepdims=True) + EPSILON)
            * norm_gain
        ).astype(jnp.bfloat16)
        pieces = (
            lax.all_gather(w_conv_gate, "sp", axis=0, tiled=True),
            lax.all_gather(w_conv_mult, "sp", axis=0, tiled=True),
            lax.all_gather(w_conv_in, "sp", axis=0, tiled=True),
            lax.all_gather(w_query, "sp", axis=0, tiled=True),
            lax.all_gather(w_key, "sp", axis=0, tiled=True),
            lax.all_gather(w_value, "sp", axis=0, tiled=True),
        )
        projected = tuple(
            (jnp.dot(normed, shard_piece, preferred_element_type=jnp.float32) for shard_piece in pieces)
        )
        conv_gate, conv_mult, conv_in, query, keys_proj, value = [
            tensor.astype(jnp.bfloat16).reshape(seq_count, tokens, -1) for tensor in projected
        ]
        entry_cols = lax.dynamic_slice_in_dim(w_input_gate, group_index * heads_here, heads_here, 1)
        forget_cols = lax.dynamic_slice_in_dim(w_forget_gate, group_index * heads_here, heads_here, 1)
        gate_values = jnp.dot(
            normed,
            jnp.concatenate([entry_cols, forget_cols], axis=1),
            preferred_element_type=jnp.float32,
        ).reshape(seq_count, tokens, 2 * heads_here)
    product = (conv_mult.astype(jnp.float32) * conv_in.astype(jnp.float32)).astype(jnp.bfloat16)
    ntaps = conv_taps.shape[0]
    rim_rows = from_behind(product[:, tokens - (ntaps - 1) :, :], "sp", 1)
    padded = jnp.concatenate([rim_rows, product], axis=1).astype(jnp.float32)
    tap_weights = lax.dynamic_slice_in_dim(conv_taps, group_index * channels, channels, 1)
    mixed_sum = jnp.zeros((seq_count, tokens, channels), jnp.float32)
    for tap_index in range(ntaps):
        mixed_sum = (
            mixed_sum + tap_weights[tap_index] * padded[:, tap_index : tap_index + tokens, :]
        )
    conv_out = (conv_gate.astype(jnp.float32) * mixed_sum).astype(jnp.bfloat16)
    bias_rows = lax.dynamic_slice_in_dim(gate_bias, group_index * heads_here, heads_here, 1)
    decay_rows = lax.dynamic_slice_in_dim(decay_shift, group_index * heads_here, heads_here, 2)
    entry = gate_values[..., :heads_here] + bias_rows[0]
    log_forget = jax.nn.log_sigmoid(gate_values[..., heads_here:] + bias_rows[1]) + decay_rows
    cell = memory_cell(
        head_rows(query, seq_count, heads_here),
        head_rows(keys_proj, seq_count, heads_here),
        head_rows(value, seq_count, heads_here),
        gate_rows(entry, seq_count, heads_here),
        gate_rows(log_forget, seq_count, heads_here),
    )
    cell = cell * lax.rsqrt(jnp.mean(cell * cell, axis=-1, keepdims=True) + EPSILON)
    gain_rows = lax.dynamic_slice_in_dim(
        head_gain, group_index * heads_here * HEAD_DIM, heads_here * HEAD_DIM, 0
    ).reshape(1, heads_here, 1, HEAD_DIM)
    scaled = cell.reshape(seq_count, heads_here, tokens, HEAD_DIM) * gain_rows
    mem_out = (
        scaled.transpose(0, 2, 1, 3)
        .reshape(seq_count, tokens, heads_here * HEAD_DIM)
        .astype(jnp.bfloat16)
    )
    if full_out is not None:
        mix = jnp.stack([conv_out, mem_out]).reshape(2, seq_count * 2, tokens // 2, channels)
        merged = exchange_and_merge(mix.transpose(1, 0, 2, 3), full_out)
        return merged[None]
    conv_seq, mem_seq = (
        lax.all_to_all(conv_out, "fs", split_axis=0, concat_axis=2, tiled=True),
        lax.all_to_all(mem_out, "fs", split_axis=0, concat_axis=2, tiled=True),
    )
    rows_conv, rows_mem = (
        lax.all_gather(w_out_conv, "fs", axis=0, tiled=True),
        lax.all_gather(w_out_mem, "fs", axis=0, tiled=True),
    )
    full_conv, full_mem = (
        lax.all_gather(rows_conv, "sp", axis=1, tiled=True),
        lax.all_gather(rows_mem, "sp", axis=1, tiled=True),
    )
    conv_flat = conv_seq[0]
    mem_flat = mem_seq[0]
    output = lax.psum_scatter(
        (
            jnp.dot(conv_flat, full_conv, preferred_element_type=jnp.float32)
            + jnp.dot(mem_flat, full_mem, preferred_element_type=jnp.float32)
        ).astype(jnp.bfloat16),
        "tp",
        scatter_dimension=0,
        tiled=True,
    ).astype(jnp.float32)
    return output.astype(jnp.bfloat16).reshape(1, output.shape[0], -1)


def solution(mesh):
    return jax.shard_map(
        shards,
        mesh=mesh,
        in_specs=(
            P("fs", "sp", None),
            P(),
            P("sp", ("fs", "tp")),
            P("sp", ("fs", "tp")),
            P("sp", ("fs", "tp")),
            P(),
            P("sp", ("fs", "tp")),
            P("sp", ("fs", "tp")),
            P("sp", ("fs", "tp")),
            P(),
            P(),
            P(),
            P(None, "sp", None),
            P(),
            P(("fs", "tp"), "sp"),
            P(("fs", "tp"), "sp"),
        ),
        out_specs=P("fs", ("sp", "tp"), None),
        check_vma=False,
    )
```

profile of v0, /device:TPU:25, one launch (start us, length us, event | category | flops | bytes accessed | tf_op | source)
XLA Modules:
  0.0 151.3 jit_solution(4424998440761914225)
XLA Ops:
  0.0 0.8 pad_maximum_fusion
  1.1 1.2 copy-done.2
  2.3 0.9 copy-done.3
  3.2 0.9 copy-done.4
  4.1 0.9 copy-done.5
  5.0 0.9 copy-done.6
  5.9 0.9 copy-done.7
  6.8 0.9 copy-done.8
  7.7 0.9 copy-done.9
  8.6 0.9 copy-done.10
  9.5 0.7 copy-done.11
  10.2 82.6 %shard_map.154 = (bf16[1024,768]{1,0:T(8,128)(2,1)}, f32[1024,16]{1,0:T(8,128)S(1)}, bf16[8,2,128,2048]{3,2,1,0:T(8,128)(2,1)}) custom-call(bf16[256,2048]{1,0:T(8,128)(2,1)S(1)} %bitcast.127, f32[1,2048]{1,0:T(1,128)S(1)} %bitcast.128, bf16[512,128]{1,0:T(8,128)(2,1)S(1)} %copy-done.3, bf16[512,128]{1,0:T(8,128)(2,1)S(1)} %copy-done.4, ...), custom_call_target="tpu_custom_call" | custom-call | tf_op jit(solution)/shard_map/pallas_call | solution.py:518
  92.9 1.3 multiply_convert_fusion.1
  94.3 1.5 collective-permute-start
  95.9 0.8 fusion.39
  98.1 1.4 fusion.33
  99.6 0.9 reduce_window_sum.11
  101.8 2.0 %convolution_bitcast_fusion = f32[4,4,128,128]{3,2,0,1:T(8,128)S(1)} fusion(f32[4,4,64,128]{3,2,1,0:T(8,128)S(1)} %bitcast.129, bf16[4,4,64,128]{3,2,1,0:T(8,128)(2,1)S(1)} %bitcast.131, f32[4,4,64]{2,1,0:T(4,128)S(1)} %subtract_exponential_fusion.3), kind=kOutput, calls=%fused_computation.16 | convolution fusion | flops 201588736 | bytes 1839104 | tf_op jit(solution)/shard_map/bclv,bclk->bcvk/dot_general | solution.py:147
  103.8 3.9 %while.21 = (s32[]{:T(128)}, f32[4]{0:T(128)S(1)}, f32[4]{0:T(128)S(1)}, f32[4,128,128]{2,1,0:T(8,128)S(1)}, f32[4,4]{1,0:T(4,128)S(1)}, /*index=5*/f32[4,4]{1,0...) while((s32[]{:T(128)}, f32[4]{0:T(128)S(1)}, ...), condition=%wide.region_3.4_spmd.clone, body=%wide.region_2.3_spmd.clone.sunk | while | flops 327711 | bytes 1311169 | solution.py:165
  103.9 0.7 bitcast_dynamic-update-slice_fusion.2
  104.9 0.7 bitcast_dynamic-update-slice_fusion.2
  105.9 0.7 bitcast_dynamic-update-slice_fusion.2
  106.9 0.7 bitcast_dynamic-update-slice_fusion.2
  108.5 0.7 convert_element_type.65.state_ref
  109.2 18.1 %shard_map.155 = (bf16[4,4,128,128]{3,2,1,0:T(8,128)(2,1)}, f32[4,4,8,128]{3,2,1,0:T(8,128)}) custom-call(bf16[4,128,128]{2,1,0:T(8,128)(2,1)} %convert_element_type.65.state_ref, f32[4,8,128]{2,1,0:T(8,128)} %pad.4.stat_ref), custom_call_target="tpu_custom_call" | custom-call | tf_op jit(solution)/shard_map/pallas_call | solution.py:61
  127.3 1.0 slice_reduce_fusion.1
  128.5 0.8 dynamic_slice.34
  131.1 0.9 copy-done.15
  131.9 1.3 multiply_reduce_fusion
  133.9 3.4 %copy-done.1 = bf16[8,2,128,2048]{3,2,1,0:T(8,128)(2,1)S(1)} copy-done((bf16[8,2,128,2048]{3,2,1,0:T(8,128)(2,1)S(1)}, bf16[8,2,128,2048]{3,2,1,0:T(8,128)(2,1)}, u32[]{:S(2)}) %copy-start.1) | copy-done | bytes 8388632
  137.3 13.2 %shard_map.156 = bf16[128,2048]{1,0:T(8,128)(2,1)S(1)} custom-call(bf16[8,2,128,128]{3,2,1,0:T(8,128)(2,1)S(1)} %maximum_bitcast_fusion.mix_ref, bf16[8,2,128,2048]{3,2,1,0:T(8,128)(2,1)S(1)} %copy-done.1), custom_call_target="tpu_custom_call" | custom-call | tf_op jit(solution)/shard_map/pallas_call | solution.py:609
  150.5 0.8 copy.76
  (95 shorter events, 7.2 us)
Async XLA Ops:
  0.0 129.2 %copy-start = (f32[3,1024]{1,0:T(4,128)S(1)}, f32[3,1024]{1,0:T(4,128)}, u32[]{:S(2)}) copy-start(f32[3,1024]{1,0:T(4,128)} %param.23) | copy-start | bytes 36868
  1.1 1.2 copy-start.2
  2.3 0.9 copy-start.3
  3.2 0.9 copy-start.4
  4.1 0.9 copy-start.5
  5.0 0.9 copy-start.6
  5.9 0.9 copy-start.7
  6.8 0.9 copy-start.8
  7.7 0.9 copy-start.9
  8.6 0.9 copy-start.10
  9.5 0.7 copy-start.11
  92.9 3.0 %copy-start.12 = (bf16[1024,768]{1,0:T(8,128)(2,1)S(1)}, bf16[1024,768]{1,0:T(8,128)(2,1)}, u32[]{:S(2)}) copy-start(bf16[1024,768]{1,0:T(8,128)(2,1)} %get-tuple-element.67) | copy-start | bytes 4718596
  92.9 3.8 %copy-start.18 = (f32[2,8]{1,0:T(2,128)S(1)}, f32[2,8]{1,0:T(2,128)}, u32[]{:S(2)}) copy-start(f32[2,8]{1,0:T(2,128)} %param.29) | copy-start | bytes 196
  94.3 1.6 %copy-start.13 = (bf16[1024,128]{1,0:T(8,128)(2,1)}, bf16[1024,128]{1,0:T(8,128)(2,1)S(1)}, u32[]{:S(2)}) copy-start(bf16[1024,128]{1,0:T(8,128)(2,1)S(1)} %get-tuple-element.183) | copy-start | bytes 786436
  94.3 39.3 %collective-permute-start = (bf16[4,2,128]{2,1,0:T(2,128)(2,1)S(1)}, bf16[4,2,128]{2,1,0:T(2,128)(2,1)S(1)}, u32[]{:S(2)}, u32[]{:S(2)}) collective-permute-start(bf16[4,2,128]{2,1,0:T(2,128)(2,1)S(1)} %slice.122), channel_id=1, source_target_pairs={{0,8},{8,16},{16,24},{1,9},{9,17},{17,25},{2,10},{10,18},{18,26},{... | collective-permute-start | bytes 6152 | tf_op jit(solution)/shard_map/ppermute | solution.py:105
  127.3 3.4 %copy-start.17 = (bf16[4,4,128,128]{3,2,1,0:T(8,128)(2,1)S(1)}, bf16[4,4,128,128]{3,2,1,0:T(8,128)(2,1)}, u32[]{:S(2)}) copy-start(bf16[4,4,128,128]{3,2,1,0:T(8,128)(2,1)} %get-tuple-element.75) | copy-start | bytes 1572868
  130.7 1.2 copy-start.15
  131.9 1.6 %copy-start.14 = (bf16[1024,128]{1,0:T(8,128)(2,1)S(1)}, bf16[1024,128]{1,0:T(8,128)(2,1)}, u32[]{:S(2)}) copy-start(bf16[1024,128]{1,0:T(8,128)(2,1)} %copy-done.13) | copy-start | bytes 786436
  131.9 1.7 %copy-start.16 = (bf16[1024,128]{1,0:T(8,128)(2,1)S(1)}, bf16[1024,128]{1,0:T(8,128)(2,1)}, u32[]{:S(2)}) copy-start(bf16[1024,128]{1,0:T(8,128)(2,1)} %get-tuple-element.180) | copy-start | bytes 786436
  133.9 3.4 %copy-start.1 = (bf16[8,2,128,2048]{3,2,1,0:T(8,128)(2,1)S(1)}, bf16[8,2,128,2048]{3,2,1,0:T(8,128)(2,1)}, u32[]{:S(2)}) copy-start(bf16[8,2,128,2048]{3,2,1,0:T(8,128)(2,1)} %get-tuple-element.77.wo_ref) | copy-start | bytes 25165828
where the time goes:
time: 152 us; the launch traced here: 151 us
  Pallas kernels  114 us (75%)
  local copies, waits for them, and re-layouts  19.2 us (13%)
  other arithmetic  11.9 us (8%)
  matrix products  4.22 us (3%)
    pallas_call x1, Pallas kernels, gather_and_project(): pl.pallas_call(functools.partial(gather_kernel, ns, nf, cuts), out_shape=...  82.6 us
    pallas_call x1, Pallas kernels, send_later(): pl.pallas_call(functools.partial(later_kernel, ns), out_shape=(jax.ShapeD...  18.1 us
    unnamed x41, local copies, waits for them, and re-layouts  14.4 us
    pallas_call x1, Pallas kernels, exchange_and_merge(): pl.pallas_call(functools.partial(output_kernel, nf), out_shape=jax.ShapeD...  13.2 us
  transfers between devices with their start and end apart: 1, of which 0 were waited for; matrix products, arithmetic and copies ran while one was open for 12% of the time, Pallas kernels for 12%

commit v1 on v0

v1 whole, which is shorter than its diff:
```python
import functools

import jax
import jax.numpy as jnp
from jax import lax
from jax.experimental import pallas as pl
from jax.experimental.pallas import tpu as pltpu
from jax.sharding import PartitionSpec as P

MEMORY_HEADS = 8
HEAD_DIM = 128
BLOCK = 64


EPSILON = 1e-06
FAR_BELOW = -1e30
HIGHEST_PRECISION = lax.Precision.HIGHEST


def prefix(value, axis, join, neutral):
    count, mine = (lax.axis_size(axis), lax.axis_index(axis))
    total, peak, state = value
    stats = jnp.stack([total, peak], axis=1)[..., None]
    stats = jnp.broadcast_to(stats, stats.shape[:2] + state.shape[-1:])
    packed = lax.all_gather(jnp.concatenate([state, stats], axis=1), axis)
    height = state.shape[1]
    pieces = (packed[:, :, height, 0], packed[:, :, height + 1, 0], packed[:, :, :height])
    subtotal = jax.tree.map(
        lambda part, zero: jnp.full_like(part, 0) + jnp.asarray(zero, part.dtype), value, neutral
    )

    def lap(position, subtotal):
        longer = join(subtotal, jax.tree.map(lambda part: part[position], pieces))
        return jax.tree.map(lambda new, old: jnp.where(position < mine, new, old), longer, subtotal)

    return lax.fori_loop(0, count - 1, lap, subtotal)


def from_behind(array, axis, by):
    peers = lax.axis_size(axis)
    pairs = [(i, i + by) for i in range(peers) if 0 <= i + by < peers]
    return lax.ppermute(array, axis, pairs)


def combine_states(earlier, later):
    total_one, peak_one, state_one = earlier
    total_two, peak_two, state_two = later
    peak_new = jnp.maximum(total_two + peak_one, peak_two)
    scale_old = jnp.exp(total_two + peak_one - peak_new)
    scale_new = jnp.exp(peak_two - peak_new)
    return (
        total_one + total_two,
        peak_new,
        scale_old[..., None, None] * state_one + scale_new[..., None, None] * state_two,
    )


def head_rows(values, seq_count, heads_here):
    tokens = values.shape[1]
    split_heads = values.reshape(seq_count, tokens, heads_here, HEAD_DIM).transpose(0, 2, 1, 3)
    return split_heads.reshape(seq_count * heads_here, tokens, HEAD_DIM).astype(jnp.float32)


def gate_rows(values, seq_count, heads_here):
    tokens = values.shape[1]
    return values.transpose(0, 2, 1).reshape(seq_count * heads_here, tokens)


def memory_cell(query_rows, key_rows, value_rows, entry_gate, log_forget):
    members = query_rows.shape[0]
    tokens = query_rows.shape[1]
    head_width = query_rows.shape[2]
    nblocks = tokens // BLOCK
    block_shape = (members, nblocks, BLOCK, head_width)
    query_blocks = query_rows.reshape(block_shape)
    key_blocks = key_rows.reshape(block_shape) * head_width ** (-0.5)
    value_blocks = value_rows.reshape(block_shape)
    entry_blocks = entry_gate.reshape(members, nblocks, BLOCK)
    forget_sums = jnp.cumsum(log_forget.reshape(members, nblocks, BLOCK), axis=-1)
    block_total = forget_sums[..., -1]
    local_logs = block_total[..., None] - forget_sums + entry_blocks
    local_peak = jnp.max(local_logs, axis=-1)
    local_weights = jnp.exp(local_logs - local_peak[..., None])
    local_state = jnp.einsum(
        "bclv,bclk->bcvk",
        local_weights[..., None] * value_blocks,
        key_blocks,
        precision=HIGHEST_PRECISION,
    )

    def advance(running, block_item):
        return (combine_states(running, block_item), running)

    zero_sums = jnp.zeros((members,), jnp.float32)
    low_peaks = jnp.full((members,), FAR_BELOW, jnp.float32)
    zero_states = jnp.zeros((members, head_width, head_width), jnp.float32)
    block_items = (
        jnp.moveaxis(block_total, 1, 0),
        jnp.moveaxis(local_peak, 1, 0),
        jnp.moveaxis(local_state, 1, 0),
    )
    device_total, inner_states = lax.scan(advance, (zero_sums, low_peaks, zero_states), block_items)
    inner_states = tuple((jnp.moveaxis(tensor, 0, 1) for tensor in inner_states))
    total_sum, total_peak, total_state = device_total
    before = prefix(
        (total_sum, total_peak, total_state),
        "sp",
        combine_states,
        (zero_sums, low_peaks, zero_states),
    )
    opening = combine_states((zero_sums, zero_sums, zero_states), before)
    opening = tuple((tensor[:, None] for tensor in opening))
    _, prior_peak, prior_state = combine_states(opening, inner_states)
    positions = jnp.arange(BLOCK)
    causal_mask = positions[:, None] >= positions[None, :]
    pair_logs = jnp.where(
        causal_mask,
        forget_sums[..., :, None] - forget_sums[..., None, :] + entry_blocks[..., None, :],
        -jnp.inf,
    )
    carried_logs = forget_sums + prior_peak[..., None]
    row_peak = jnp.maximum(carried_logs, jnp.max(pair_logs, axis=-1))
    inner_weights = jnp.exp(pair_logs - row_peak[..., None])
    carried_weights = jnp.exp(carried_logs - row_peak)
    scores = inner_weights * jnp.einsum(
        "bcld,bcsd->bcls", query_blocks, key_blocks, precision=HIGHEST_PRECISION
    )
    numerator = carried_weights[..., None] * jnp.einsum(
        "bcvk,bclk->bclv", prior_state, query_blocks, precision=HIGHEST_PRECISION
    ) + jnp.einsum("bcls,bcsv->bclv", scores, value_blocks, precision=HIGHEST_PRECISION)
    return numerator.reshape(members, tokens, head_width)


MESH = pl.DeviceIdType.MESH
F32 = jnp.float32
BF16 = jnp.bfloat16
TAPS = 3
RIM = 8
KV, QUERY, OUT, MIX, GATE = range(5)
SPANS = {KV: (0, 2), QUERY: (2, 1), MIX: (3, 2), GATE: (5, 1)}
PARTS = 5


def layer_kernel(
    ns,
    nf,
    act_ref,
    gain_ref,
    w0_ref,
    w1_ref,
    w2_ref,
    w3_ref,
    w4_ref,
    w5_ref,
    wi_ref,
    wf_ref,
    bias_ref,
    decay_ref,
    taps_ref,
    head_ref,
    wc_ref,
    wm_ref,
    out_ref,
    raw,
    gain,
    normed,
    wbuf,
    wi,
    wf,
    bias,
    decay,
    taps,
    head,
    wo,
    kv,
    query,
    logs,
    logs_t,
    local_state,
    local_stat,
    carry,
    carry_m,
    passed,
    passed_m,
    padded,
    mixed,
    gate_sum,
    mine,
    got,
    acc,
    other,
    load_sem,
    x_send,
    x_recv,
    d_send,
    d_recv,
    w_send,
    w_recv,
    p_send,
    p_recv,
    s_send,
    s_recv,
    r_send,
    r_recv,
    m_send,
    m_recv,
    e_send,
    e_recv,
):
    sp, fs, tp = (lax.axis_index("sp"), lax.axis_index("fs"), lax.axis_index("tp"))
    g = fs * 2 + tp
    depth, cols = w0_ref.shape
    half, model = raw.shape
    tokens = 2 * half
    ocols = wc_ref.shape[1]
    partner = (sp, fs, 1 - tp)
    has_up, has_down = (sp + 1 < ns, sp > 0)
    up, down = ((sp + 1, fs, tp), (sp - 1, fs, tp))
    fy, fx = (fs // 2, lax.rem(fs, 2))
    ny = nf // 2

    def ahead(k):
        return lax.rem(fy + k // 2, ny) * 2 + lax.rem(fx + k % 2, 2)

    def behind(k):
        return lax.rem(fy + ny - k // 2, ny) * 2 + lax.rem(fx + k % 2, 2)

    def block(index, size):
        return pl.ds(pl.multiple_of(index * size, size), size)

    def remote(src, dst, send, recv, to):
        return pltpu.make_async_remote_copy(
            src, dst, send, recv, device_id=to, device_id_type=MESH
        )

    loads = [pltpu.make_async_copy(act_ref.at[block(tp, half)], raw, load_sem.at[0])]
    loads.append(pltpu.make_async_copy(gain_ref, gain, load_sem.at[1]))
    for j, ref in enumerate((w0_ref, w1_ref, w2_ref, w3_ref, w4_ref, w5_ref)):
        loads.append(
            pltpu.make_async_copy(
                ref, wbuf.at[block(sp, depth), pl.ds(j * cols, cols)], load_sem.at[2 + j]
            )
        )
    for m, ref in enumerate((wc_ref, wm_ref)):
        loads.append(
            pltpu.make_async_copy(
                ref, wo.at[m, block(fs, cols), block(sp, ocols)], load_sem.at[8 + m]
            )
        )
    smalls = (
        (wi_ref, wi),
        (wf_ref, wf),
        (bias_ref, bias),
        (decay_ref, decay),
        (taps_ref, taps),
        (head_ref, head),
    )
    for j, (ref, held) in enumerate(smalls):
        loads.append(pltpu.make_async_copy(ref, held, load_sem.at[10 + j]))
    for j in (2, 3, 0, 1, 4, 8, 9, 5, 6, 7, 10, 11, 12, 13, 14, 15):
        loads[j].start()

    barrier = pltpu.get_barrier_semaphore()
    for k in range(1, nf):
        pl.semaphore_signal(barrier, inc=1, device_id=(sp, ahead(k), tp), device_id_type=MESH)
    pl.semaphore_signal(barrier, inc=1, device_id=partner, device_id_type=MESH)

    @pl.when(has_up)
    def _():
        pl.semaphore_signal(barrier, inc=1, device_id=up, device_id_type=MESH)

    @pl.when(has_down)
    def _():
        pl.semaphore_signal(barrier, inc=1, device_id=down, device_id_type=MESH)

    def place(part, owner):
        if part == OUT:
            return wo.at[:, block(fs, cols), block(owner, ocols)]
        first, count = SPANS[part]
        return wbuf.at[block(owner, depth), pl.ds(first * cols, count * cols)]

    def z_copy(part, side, d, owner):
        there = place(part, owner)
        return remote(
            there,
            there,
            w_send.at[side, d, part],
            w_recv.at[side, d, part],
            (up, down)[side],
        )

    def owner_of(side, d):
        return sp - d if side == 0 else sp + d

    def arrives(side, d):
        return (sp - d >= 0) if side == 0 else (sp + d < ns)

    def sends(side, d):
        return arrives(side, d) & (has_up if side == 0 else has_down)

    def z_send(part, side, d):
        @pl.when(sends(side, d))
        def _():
            z_copy(part, side, d, owner_of(side, d)).start()

    def own(part):
        for side in range(2):
            z_send(part, side, 0)

    def p_copy(owner, k, row):
        there = wo.at[:, block(row, cols), block(owner, ocols)]
        return remote(
            there, there, p_send.at[owner, k - 1], p_recv.at[owner, k - 1], (sp, ahead(k), tp)
        )

    def spread(owner):
        for k in range(1, nf):
            p_copy(owner, k, fs).start()

    def z_step(part, d, use=None):
        for side in range(2):

            @pl.when(arrives(side, d))
            def _():
                owner = owner_of(side, d)
                z_copy(part, side, d - 1, owner).wait_recv()
                if d < ns - 1:
                    z_send(part, side, d)
                if part == OUT:
                    spread(owner)
                if use is not None:
                    use(owner)

    def x_copy(k, seq):
        there = normed.at[pl.ds(pl.multiple_of(seq * tokens + tp * half, half), half)]
        return remote(there, there, x_send.at[k - 1], x_recv.at[k - 1], (sp, ahead(k), tp))

    def d_copy(k, seq, part):
        there = normed.at[pl.ds(pl.multiple_of(seq * tokens + part * half, half), half)]
        return remote(there, there, d_send.at[k], d_recv.at[k], partner)

    loads[2].wait()
    loads[3].wait()
    pl.semaphore_wait(barrier, nf + has_up.astype(jnp.int32) + has_down.astype(jnp.int32))
    own(KV)
    loads[0].wait()
    loads[1].wait()
    step = 32

    def norm_rows(i, carried):
        x = raw[pl.ds(pl.multiple_of(i * step, step), step), :].astype(F32)
        scale = lax.rsqrt(jnp.mean(x * x, axis=-1, keepdims=True) + EPSILON)
        rows = pl.ds(pl.multiple_of(fs * tokens + tp * half + i * step, step), step)
        normed[rows, :] = (x * scale * gain[...]).astype(BF16)
        return carried

    lax.fori_loop(0, half // step, norm_rows, 0)
    loads[4].wait()
    own(QUERY)
    for k in range(1, nf):
        x_copy(k, fs).start()
    d_copy(0, fs, tp).start()
    loads[8].wait()
    loads[9].wait()
    z_step(KV, 1)

    def relay(k):
        x_copy(k, behind(k)).wait_recv()
        d_copy(k, behind(k), tp).start()

    for k in range(1, nf - 1):
        relay(k)
    for d in range(2, ns - 1):
        z_step(KV, d)
    own(OUT)
    spread(sp)
    relay(nf - 1)
    for d in range(1, ns - 1):
        z_step(QUERY, d)
    for j in (5, 6, 7, 10, 11, 12, 13, 14, 15):
        loads[j].wait()
    own(MIX)
    z_step(KV, ns - 1)
    for k in range(nf):
        d_copy(k, behind(k), 1 - tp).wait_recv()

    def tile(i):
        return pl.ds(pl.multiple_of(i * tokens, tokens), tokens)

    def project(part, into):
        first, count = SPANS[part]

        def body(i, carried):
            into[tile(i), :] = jnp.dot(
                normed[tile(i), :],
                wbuf[:, first * cols : (first + count) * cols],
                preferred_element_type=F32,
            ).astype(BF16)
            return carried

        lax.fori_loop(0, nf, body, 0)

    lane8 = lax.broadcasted_iota(jnp.int32, (tokens, wi.shape[1]), 1)
    lane = lax.broadcasted_iota(jnp.int32, (tokens, 128), 1)
    row_at = lax.broadcasted_iota(jnp.int32, (tokens, tokens), 0)
    col_at = lax.broadcasted_iota(jnp.int32, (tokens, tokens), 1)
    packed = jnp.zeros((tokens, 128), F32)
    for s in range(nf):
        x = normed[s * tokens : (s + 1) * tokens, :]
        entry = jnp.dot(x, wi[...], preferred_element_type=F32) + bias[0:1, :]
        raw_forget = jnp.dot(x, wf[...], preferred_element_type=F32) + bias[1:2, :]
        forget = (
            jnp.minimum(raw_forget, 0.0) - jnp.log1p(jnp.exp(-jnp.abs(raw_forget))) + decay[s]
        )
        entry = jnp.sum(jnp.where(lane8 == g, entry, 0.0), axis=1, keepdims=True)
        forget = jnp.sum(jnp.where(lane8 == g, forget, 0.0), axis=1, keepdims=True)
        packed = jnp.where(lane == s, forget, packed)
        packed = jnp.where(lane == nf + s, entry, packed)
    ones = jnp.where(row_at >= col_at, 1.0, 0.0).astype(F32)
    sums = jnp.dot(ones, packed, precision=HIGHEST_PRECISION, preferred_element_type=F32)
    sums = jnp.where(lane < nf, sums, packed)
    logs[...] = sums
    logs_t[...] = sums.T
    project(KV, kv)
    for s in range(nf):
        rows = pl.ds(s * tokens, tokens)
        total = logs_t[s : s + 1, tokens - 1 : tokens]
        reach = total - logs[:, s : s + 1] + logs[:, nf + s : nf + s + 1]
        peak = jnp.max(reach, axis=0, keepdims=True)
        weighted = (kv[rows, cols:].astype(F32) * jnp.exp(reach - peak)).astype(BF16)
        local_state[s] = lax.dot_general(
            kv[rows, :cols], weighted, (((0,), (0,)), ((), ())), preferred_element_type=F32
        )
        local_stat[s : s + 1, :] = jnp.broadcast_to(total, (1, 128))
        local_stat[nf + s : nf + s + 1, :] = jnp.broadcast_to(peak, (1, 128))

    z_step(QUERY, ns - 1)
    z_step(OUT, 1)

    def state_copies():
        return (
            remote(passed_m, carry_m, s_send.at[0], s_recv.at[0], up),
            remote(passed, carry, s_send.at[1], s_recv.at[1], up),
        )

    @pl.when(jnp.logical_not(has_down))
    def _():
        carry[...] = jnp.zeros_like(carry)
        carry_m[...] = jnp.zeros_like(carry_m)

    @pl.when(has_down)
    def _():
        for copy in state_copies():
            copy.wait_recv()

    @pl.when(has_up)
    def _():
        for s in range(nf):
            before = local_stat[s : s + 1, :] + carry_m[s : s + 1, :]
            peak = local_stat[nf + s : nf + s + 1, :]
            top = jnp.maximum(before, peak)
            passed[s] = (
                jnp.exp(before - top) * carry[s].astype(F32) + jnp.exp(peak - top) * local_state[s]
            ).astype(BF16)
            passed_m[s : s + 1, :] = top
        for copy in state_copies():
            copy.start()

    for d in range(2, ns - 1):
        z_step(OUT, d)
    own(GATE)
    project(QUERY, query)

    def mix_copy(m, k, seq, source):
        return remote(
            mine.at[m, seq],
            got.at[m, :, block(source, cols)],
            m_send.at[m, k - 1],
            m_recv.at[m, k - 1],
            (sp, ahead(k), tp),
        )

    def hand_out(m):
        for k in range(1, nf):
            mix_copy(m, k, ahead(k), fs).start()
        got[m, :, block(fs, cols)] = mine[m, fs]

    scale = HEAD_DIM ** (-0.5)
    head_gain = head[:, block(g, cols)]
    causal = row_at >= col_at
    for s in range(nf):
        rows = pl.ds(s * tokens, tokens)
        scores = lax.dot_general(
            query[rows, :], kv[rows, :cols], (((1,), (1,)), ((), ())), preferred_element_type=F32
        )
        sums = logs[:, s : s + 1]
        pairs = jnp.where(
            causal,
            sums - logs_t[s : s + 1, :] + logs_t[nf + s : nf + s + 1, :],
            FAR_BELOW,
        )
        carried = sums + carry_m[s : s + 1, 0:1]
        top = jnp.maximum(carried, jnp.max(pairs, axis=1, keepdims=True))
        weights = (jnp.exp(pairs - top) * scores).astype(BF16)
        cell = jnp.dot(weights, kv[rows, cols:], preferred_element_type=F32)
        cell = cell + jnp.exp(carried - top) * jnp.dot(
            query[rows, :], carry[s], preferred_element_type=F32
        )
        cell = cell * scale
        cell = cell * lax.rsqrt(jnp.mean(cell * cell, axis=-1, keepdims=True) + EPSILON)
        mine[1, s] = (cell * head_gain).astype(BF16)

    for d in range(1, ns - 1):
        z_step(MIX, d)
    hand_out(1)
    z_step(OUT, ns - 1)
    z_step(MIX, ns - 1)

    def rim_copy():
        return remote(
            padded.at[:, pl.ds(tokens, RIM), :],
            padded.at[:, pl.ds(0, RIM), :],
            r_send,
            r_recv,
            up,
        )

    def product(i, carried):
        both = jnp.dot(
            normed[tile(i), :],
            wbuf[:, SPANS[MIX][0] * cols : SPANS[GATE][0] * cols],
            preferred_element_type=F32,
        ).astype(BF16)
        both = both.astype(F32)
        padded[i, RIM:, :] = (both[:, :cols] * both[:, cols:]).astype(BF16).astype(F32)
        return carried

    lax.fori_loop(0, nf, product, 0)

    @pl.when(jnp.logical_not(has_down))
    def _():
        padded[:, 0:RIM, :] = jnp.zeros((nf, RIM, cols), F32)

    @pl.when(has_up)
    def _():
        rim_copy().start()

    gate_first, gate_count = SPANS[GATE]

    def gate_part(owner, first=False):
        def body(i, carried):
            part = jnp.dot(
                normed[tile(i), block(owner, depth)],
                wbuf[block(owner, depth), gate_first * cols : (gate_first + gate_count) * cols],
                preferred_element_type=F32,
            )
            gate_sum[tile(i), :] = part if first else gate_sum[tile(i), :] + part
            return carried

        lax.fori_loop(0, nf, body, 0)

    gate_part(sp, True)
    for d in range(1, ns - 1):
        z_step(GATE, d, gate_part)

    @pl.when(has_down)
    def _():
        rim_copy().wait_recv()

    tap = taps[:, block(g, cols)]
    for s in range(nf):
        total = jnp.zeros((tokens, cols), F32)
        for j in range(TAPS):
            at = RIM - (TAPS - 1) + j
            total = total + tap[j : j + 1, :] * padded[s, at : at + tokens, :]
        mixed[s * tokens : (s + 1) * tokens, :] = total

    def arrived(owner, carried):
        for k in range(1, nf):
            p_copy(owner, k, behind(k)).wait_recv()
        return carried

    lax.fori_loop(0, ns, arrived, 0)
    for k in range(1, nf):
        mix_copy(1, k, ahead(k), behind(k)).wait_recv()

    def memory_share(i, carried):
        acc[:, block(i, ocols)] = jnp.dot(
            got[1], wo[1, :, block(i, ocols)], preferred_element_type=F32
        )
        return carried

    lax.fori_loop(0, ns, memory_share, 0)

    z_step(GATE, ns - 1, gate_part)
    for s in range(nf):
        rows = slice(s * tokens, (s + 1) * tokens)
        mine[0, s] = (gate_sum[rows, :].astype(BF16).astype(F32) * mixed[rows, :]).astype(BF16)
    hand_out(0)
    for k in range(1, nf):
        mix_copy(0, k, ahead(k), behind(k)).wait_recv()

    def e_copy(i):
        return remote(
            acc.at[block(1 - tp, half), block(i, ocols)],
            other.at[:, block(i, ocols)],
            e_send.at[i],
            e_recv.at[i],
            partner,
        )

    def finish(i, carried):
        acc[:, block(i, ocols)] = acc[:, block(i, ocols)] + jnp.dot(
            got[0], wo[0, :, block(i, ocols)], preferred_element_type=F32
        )
        e_copy(i).start()
        return carried

    lax.fori_loop(0, ns, finish, 0)

    def merge(i, carried):
        e_copy(i).wait_recv()
        out_ref[:, block(i, ocols)] = (
            acc[block(tp, half), block(i, ocols)] + other[:, block(i, ocols)]
        ).astype(BF16)
        return carried

    lax.fori_loop(0, ns, merge, 0)

    def sent(i, carried):
        e_copy(i).wait_send()
        for k in range(1, nf):
            p_copy(i, k, fs).wait_send()
        return carried

    lax.fori_loop(0, ns, sent, 0)
    for k in range(1, nf):
        x_copy(k, fs).wait_send()
        d_copy(k, behind(k), tp).wait_send()
        for m in range(2):
            mix_copy(m, k, ahead(k), fs).wait_send()
    d_copy(0, fs, tp).wait_send()
    for side in range(2):
        for d in range(ns - 1):

            @pl.when(sends(side, d))
            def _():
                for part in range(PARTS):
                    z_copy(part, side, d, owner_of(side, d)).wait_send()

    @pl.when(has_up)
    def _():
        for copy in state_copies():
            copy.wait_send()
        rim_copy().wait_send()


def whole_layer(act, gain, weights, wi, wf, bias, decay, taps, head, w_out_conv, w_out_mem):
    ns, nf = (lax.axis_size("sp"), lax.axis_size("fs"))
    tokens, model = act.shape
    half = tokens // 2
    depth, cols = weights[0].shape
    ocols = w_out_conv.shape[1]
    count = nf * tokens
    anywhere = pl.BlockSpec(memory_space=pl.ANY)
    dma = pltpu.SemaphoreType.DMA
    vmem = pltpu.VMEM
    return pl.pallas_call(
        functools.partial(layer_kernel, ns, nf),
        out_shape=jax.ShapeDtypeStruct((half, ns * ocols), BF16),
        in_specs=[anywhere] * 16,
        out_specs=pl.BlockSpec(memory_space=pltpu.VMEM),
        scratch_shapes=[
            vmem((half, model), BF16),
            vmem(gain.shape, F32),
            vmem((count, model), BF16),
            vmem((ns * depth, 6 * cols), BF16),
            vmem(wi.shape, BF16),
            vmem(wf.shape, BF16),
            vmem(bias.shape, F32),
            vmem(decay.shape, F32),
            vmem(taps.shape, F32),
            vmem(head.shape, F32),
            vmem((2, nf * cols, ns * ocols), BF16),
            vmem((count, 2 * cols), BF16),
            vmem((count, cols), BF16),
            vmem((tokens, 128), F32),
            vmem((128, tokens), F32),
            vmem((nf, cols, cols), F32),
            vmem((2 * nf, 128), F32),
            vmem((nf, cols, cols), BF16),
            vmem((8, 128), F32),
            vmem((nf, cols, cols), BF16),
            vmem((8, 128), F32),
            vmem((nf, RIM + tokens, cols), F32),
            vmem((count, cols), F32),
            vmem((count, cols), F32),
            vmem((2, nf, tokens, cols), BF16),
            vmem((2, tokens, nf * cols), BF16),
            vmem((tokens, ns * ocols), F32),
            vmem((half, ns * ocols), F32),
            dma((16,)),
            dma((nf - 1,)),
            dma((nf - 1,)),
            dma((nf,)),
            dma((nf,)),
            dma((2, ns - 1, PARTS)),
            dma((2, ns - 1, PARTS)),
            dma((ns, nf - 1)),
            dma((ns, nf - 1)),
            dma((2,)),
            dma((2,)),
            dma,
            dma,
            dma((2, nf - 1)),
            dma((2, nf - 1)),
            dma((ns,)),
            dma((ns,)),
        ],
        compiler_params=pltpu.CompilerParams(
            collective_id=0, has_side_effects=True, vmem_limit_bytes=63 * 1024 * 1024
        ),
    )(act, gain, *weights, wi, wf, bias, decay, taps, head, w_out_conv, w_out_mem)


def shards(
    activations,
    norm_gain,
    w_conv_gate,
    w_conv_mult,
    w_conv_in,
    conv_taps,
    w_query,
    w_key,
    w_value,
    w_input_gate,
    w_forget_gate,
    gate_bias,
    decay_shift,
    head_gain,
    w_out_conv,
    w_out_mem,
):
    group_index = lax.axis_index(("fs", "tp"))
    heads_here = MEMORY_HEADS // (lax.axis_size("fs") * lax.axis_size("tp"))
    channels = w_conv_gate.shape[1]
    ns, nf, nt = (lax.axis_size("sp"), lax.axis_size("fs"), lax.axis_size("tp"))
    if 2 <= ns <= 8 and nf % 2 == 0 and nt == 2 and heads_here == 1 and channels == HEAD_DIM:
        return whole_layer(
            activations[0],
            norm_gain[None, :],
            (w_key, w_value, w_query, w_conv_mult, w_conv_in, w_conv_gate),
            w_input_gate,
            w_forget_gate,
            gate_bias,
            decay_shift,
            conv_taps,
            head_gain[None, :],
            w_out_conv,
            w_out_mem,
        )[None]
    sequences = lax.all_gather(activations, "fs", axis=0, tiled=True)
    seq_count = sequences.shape[0]
    tokens = sequences.shape[1]
    model_width = sequences.shape[2]
    row_count = seq_count * tokens
    flat_rows = sequences.reshape(row_count, model_width).astype(jnp.float32)
    normed = (
        flat_rows
        * lax.rsqrt(jnp.mean(flat_rows * flat_rows, axis=-1, keepdims=True) + EPSILON)
        * norm_gain
    ).astype(jnp.bfloat16)
    pieces = (
        lax.all_gather(w_conv_gate, "sp", axis=0, tiled=True),
        lax.all_gather(w_conv_mult, "sp", axis=0, tiled=True),
        lax.all_gather(w_conv_in, "sp", axis=0, tiled=True),
        lax.all_gather(w_query, "sp", axis=0, tiled=True),
        lax.all_gather(w_key, "sp", axis=0, tiled=True),
        lax.all_gather(w_value, "sp", axis=0, tiled=True),
    )
    projected = tuple(
        (jnp.dot(normed, shard_piece, preferred_element_type=jnp.float32) for shard_piece in pieces)
    )
    conv_gate, conv_mult, conv_in, query, keys_proj, value = [
        tensor.astype(jnp.bfloat16).reshape(seq_count, tokens, -1) for tensor in projected
    ]
    entry_cols = lax.dynamic_slice_in_dim(w_input_gate, group_index * heads_here, heads_here, 1)
    forget_cols = lax.dynamic_slice_in_dim(w_forget_gate, group_index * heads_here, heads_here, 1)
    gate_values = jnp.dot(
        normed,
        jnp.concatenate([entry_cols, forget_cols], axis=1),
        preferred_element_type=jnp.float32,
    ).reshape(seq_count, tokens, 2 * heads_here)
    product = (conv_mult.astype(jnp.float32) * conv_in.astype(jnp.float32)).astype(jnp.bfloat16)
    ntaps = conv_taps.shape[0]
    rim_rows = from_behind(product[:, tokens - (ntaps - 1) :, :], "sp", 1)
    padded = jnp.concatenate([rim_rows, product], axis=1).astype(jnp.float32)
    tap_weights = lax.dynamic_slice_in_dim(conv_taps, group_index * channels, channels, 1)
    mixed_sum = jnp.zeros((seq_count, tokens, channels), jnp.float32)
    for tap_index in range(ntaps):
        mixed_sum = (
            mixed_sum + tap_weights[tap_index] * padded[:, tap_index : tap_index + tokens, :]
        )
    conv_out = (conv_gate.astype(jnp.float32) * mixed_sum).astype(jnp.bfloat16)
    bias_rows = lax.dynamic_slice_in_dim(gate_bias, group_index * heads_here, heads_here, 1)
    decay_rows = lax.dynamic_slice_in_dim(decay_shift, group_index * heads_here, heads_here, 2)
    entry = gate_values[..., :heads_here] + bias_rows[0]
    log_forget = jax.nn.log_sigmoid(gate_values[..., heads_here:] + bias_rows[1]) + decay_rows
    cell = memory_cell(
        head_rows(query, seq_count, heads_here),
        head_rows(keys_proj, seq_count, heads_here),
        head_rows(value, seq_count, heads_here),
        gate_rows(entry, seq_count, heads_here),
        gate_rows(log_forget, seq_count, heads_here),
    )
    cell = cell * lax.rsqrt(jnp.mean(cell * cell, axis=-1, keepdims=True) + EPSILON)
    gain_rows = lax.dynamic_slice_in_dim(
        head_gain, group_index * heads_here * HEAD_DIM, heads_here * HEAD_DIM, 0
    ).reshape(1, heads_here, 1, HEAD_DIM)
    scaled = cell.reshape(seq_count, heads_here, tokens, HEAD_DIM) * gain_rows
    mem_out = (
        scaled.transpose(0, 2, 1, 3)
        .reshape(seq_count, tokens, heads_here * HEAD_DIM)
        .astype(jnp.bfloat16)
    )
    conv_seq, mem_seq = (
        lax.all_to_all(conv_out, "fs", split_axis=0, concat_axis=2, tiled=True),
        lax.all_to_all(mem_out, "fs", split_axis=0, concat_axis=2, tiled=True),
    )
    rows_conv, rows_mem = (
        lax.all_gather(w_out_conv, "fs", axis=0, tiled=True),
        lax.all_gather(w_out_mem, "fs", axis=0, tiled=True),
    )
    full_conv, full_mem = (
        lax.all_gather(rows_conv, "sp", axis=1, tiled=True),
        lax.all_gather(rows_mem, "sp", axis=1, tiled=True),
    )
    conv_flat = conv_seq[0]
    mem_flat = mem_seq[0]
    output = lax.psum_scatter(
        (
            jnp.dot(conv_flat, full_conv, preferred_element_type=jnp.float32)
            + jnp.dot(mem_flat, full_mem, preferred_element_type=jnp.float32)
        ).astype(jnp.bfloat16),
        "tp",
        scatter_dimension=0,
        tiled=True,
    ).astype(jnp.float32)
    return output.astype(jnp.bfloat16).reshape(1, output.shape[0], -1)


def solution(mesh):
    return jax.shard_map(
        shards,
        mesh=mesh,
        in_specs=(
            P("fs", "sp", None),
            P(),
            P("sp", ("fs", "tp")),
            P("sp", ("fs", "tp")),
            P("sp", ("fs", "tp")),
            P(),
            P("sp", ("fs", "tp")),
            P("sp", ("fs", "tp")),
            P("sp", ("fs", "tp")),
            P(),
            P(),
            P(),
            P(None, "sp", None),
            P(),
            P(("fs", "tp"), "sp"),
            P(("fs", "tp"), "sp"),
        ),
        out_specs=P("fs", ("sp", "tp"), None),
        check_vma=False,
    )
```

time: 152 us -> 98 us (0.64)
  Pallas kernels: 114 us -> 92.1 us
  local copies, waits for them, and re-layouts: 19.2 us -> 5.64 us
  other arithmetic: 11.9 us -> 0 us
  matrix products: 4.22 us -> 0 us
    pallas_call x3 -> x1, Pallas kernels: 114 us -> 92.1 us  [whole_layer(): pl.pallas_call(functools.partial(layer_kernel, ns, nf), out_shape=jax.Sha...]
    unnamed x41 -> x8, local copies, waits for them, and re-layouts: 14.4 us -> 5.64 us
    dot_general x4 -> x0, matrix products: 4.22 us -> none  [the longest x1 1.99 us: memory_cell(): jnp.einsum('bclv,bclk->bcvk', local_weights[..., None] * value_blocks, ke...]
    dynamic_update_slice x4 -> x0, other arithmetic: 2.94 us -> none  [memory_cell(): lax.scan(advance, (zero_sums, low_peaks, zero_states), block_items)]
    add x7 -> x0, other arithmetic: 2.63 us -> none  [the longest x1 1.44 us: shards(): jax.nn.log_sigmoid(gate_values[..., heads_here:] + bias_rows[1])]
    convert_element_type x6 -> x0, other arithmetic: 2.59 us -> none  [the longest x1 1.35 us: shards(): (conv_mult.astype(jnp.float32) * conv_in.astype(jnp.float32)).astype(jnp....]
    dynamic_slice x6 -> x0, local copies, waits for them, and re-layouts: 1.55 us -> none  [the longest x1 0.76 us: shards(): lax.dynamic_slice_in_dim(head_gain, group_index * heads_here * HEAD_DIM,...]
    slice x4 -> x0, local copies, waits for them, and re-layouts: 1.54 us -> none  [the longest x1 0.84 us: shards(): flat[:, at * channels:(at + 1) * channels]]
  transfers between devices with their start and end apart: 1 -> 0, of which waited for: 0 -> 0; matrix products, arithmetic and copies ran while one was open for 12% -> 0% of each run, Pallas kernels for 12% -> 0%
where the time goes in v1:
time: 98 us; the launch traced here: 97.8 us
  Pallas kernels  92.1 us (94%)
  local copies, waits for them, and re-layouts  5.64 us (6%)
    pallas_call x1, Pallas kernels, whole_layer(): pl.pallas_call(functools.partial(layer_kernel, ns, nf), out_shape=jax.Sha...  92.1 us
    unnamed x8, local copies, waits for them, and re-layouts  5.64 us

profile of v1, /device:TPU:25, one launch (start us, length us, event | category | flops | bytes accessed | tf_op | source)
XLA Modules:
  0.0 97.8 jit_solution(4096105692134255911)
XLA Ops:
  0.0 0.0 copy-start
  0.0 1.8 %copy.17.wi_ref = bf16[2048,8]{1,0:T(8,128)(2,1)} copy(bf16[2048,8]{0,1:T(8,128)(2,1)} %param.25) | data formatting | bytes 65536 | tf_op args[9]
  1.8 0.0 copy-done
  1.8 0.0 copy-start.1
  1.8 1.0 %copy.18.wf_ref = bf16[2048,8]{1,0:T(8,128)(2,1)} copy(bf16[2048,8]{0,1:T(8,128)(2,1)S(1)} %copy-done) | data formatting | bytes 65536 | tf_op args[10]
  2.8 0.0 copy-done.1
  2.8 1.0 %copy.19.decay_ref = f32[4,256,8]{2,1,0:T(8,128)} copy(f32[4,256,8]{1,2,0:T(8,128)S(1)} %copy-done.1) | data formatting | bytes 65536 | tf_op args[12]
  3.8 92.1 %shard_map.154 = bf16[128,2048]{1,0:T(8,128)(2,1)} custom-call(bf16[256,2048]{1,0:T(8,128)(2,1)} %bitcast.5, f32[1,2048]{1,0:T(1,128)} %bitcast.6, bf16[512,128]{1,0:T(8,128)(2,1)} %w0_ref.1, bf16[512,128]{1,0:T(8,128)(2,1)} %w1_ref.1, bf16[512,128]{1,0:T(8,128)(2,1)} %w2_ref.1, bf16[512,128]{1,0:T(8,128)(2,1)} %w3_ref.1, bf16[512,128]{1,0:T(8,128)(2,1)} %w4_ref.1, ...), custom_call_target="tpu_custom_call" | custom-call | tf_op jit(solution)/shard_map/pallas_call | solution.py:668
  95.9 1.9 %copy.21 = bf16[1,128,2048]{2,1,0:T(8,128)(2,1)} copy(bf16[1,128,2048]{2,1,0:T(8,128)(2,1)} %bitcast.4) | data formatting | bytes 1048576
Async XLA Ops:
  0.0 1.8 %copy-start = (bf16[2048,8]{0,1:T(8,128)(2,1)S(1)}, bf16[2048,8]{0,1:T(8,128)(2,1)}, u32[]{:S(2)}) copy-start(bf16[2048,8]{0,1:T(8,128)(2,1)} %param.26) | copy-start | bytes 98308
  1.8 1.0 %copy-start.1 = (f32[4,256,8]{1,2,0:T(8,128)S(1)}, f32[4,256,8]{1,2,0:T(8,128)}, u32[]{:S(2)}) copy-start(f32[4,256,8]{1,2,0:T(8,128)} %param.28) | copy-start | bytes 98308

commit v2 on v1

--- a/solution.py
+++ b/solution.py
@@ -217,13 +217,7 @@
     has_up, has_down = (sp + 1 < ns, sp > 0)
     up, down = ((sp + 1, fs, tp), (sp - 1, fs, tp))
     fy, fx = (fs // 2, lax.rem(fs, 2))
-    ny = nf // 2
-
-    def ahead(k):
-        return lax.rem(fy + k // 2, ny) * 2 + lax.rem(fx + k % 2, 2)
-
-    def behind(k):
-        return lax.rem(fy + ny - k // 2, ny) * 2 + lax.rem(fx + k % 2, 2)
+    beside = (fy * 2 + 1 - fx, (1 - fy) * 2 + fx, (1 - fy) * 2 + 1 - fx)
 
     def block(index, size):
         return pl.ds(pl.multiple_of(index * size, size), size)
@@ -261,8 +255,8 @@
         loads[j].start()
 
     barrier = pltpu.get_barrier_semaphore()
-    for k in range(1, nf):
-        pl.semaphore_signal(barrier, inc=1, device_id=(sp, ahead(k), tp), device_id_type=MESH)
+    for peer in beside:
+        pl.semaphore_signal(barrier, inc=1, device_id=(sp, peer, tp), device_id_type=MESH)
     pl.semaphore_signal(barrier, inc=1, device_id=partner, device_id_type=MESH)
 
     @pl.when(has_up)
@@ -307,15 +301,32 @@
         for side in range(2):
             z_send(part, side, 0)
 
-    def p_copy(owner, k, row):
-        there = wo.at[:, block(row, cols), block(owner, ocols)]
+    def p_copy(owner, way, row):
+        span = ((0, 2), (0, 2), (0, 1), (1, 1))[way]
+        there = wo.at[pl.ds(*span), block(row, cols), block(owner, ocols)]
         return remote(
-            there, there, p_send.at[owner, k - 1], p_recv.at[owner, k - 1], (sp, ahead(k), tp)
+            there,
+            there,
+            p_send.at[owner, way],
+            p_recv.at[owner, way],
+            (sp, beside[(0, 1, 1, 0)[way]], tp),
         )
 
     def spread(owner):
-        for k in range(1, nf):
-            p_copy(owner, k, fs).start()
+        for way in range(2):
+            p_copy(owner, way, fs).start()
+
+    def pass_on(owner):
+        for way in range(2):
+            p_copy(owner, way, beside[way]).wait_recv()
+            p_copy(owner, way + 2, beside[way]).start()
+
+    def pass_step(d):
+        for side in range(2):
+
+            @pl.when(arrives(side, d))
+            def _():
+                pass_on(owner_of(side, d))
 
     def z_step(part, d, use=None):
         for side in range(2):
@@ -331,9 +342,12 @@
                 if use is not None:
                     use(owner)
 
-    def x_copy(k, seq):
-        there = normed.at[pl.ds(pl.multiple_of(seq * tokens + tp * half, half), half)]
-        return remote(there, there, x_send.at[k - 1], x_recv.at[k - 1], (sp, ahead(k), tp))
+    def x_copy(way, seq):
+        first, rows = ((0, half), (0, half), (0, half // 2), (half // 2, half // 2))[way]
+        there = normed.at[pl.ds(pl.multiple_of(seq * tokens + tp * half + first, rows), rows)]
+        return remote(
+            there, there, x_send.at[way], x_recv.at[way], (sp, beside[(0, 1, 1, 0)[way]], tp)
+        )
 
     def d_copy(k, seq, part):
         there = normed.at[pl.ds(pl.multiple_of(seq * tokens + part * half, half), half)]
@@ -357,32 +371,33 @@
     lax.fori_loop(0, half // step, norm_rows, 0)
     loads[4].wait()
     own(QUERY)
-    for k in range(1, nf):
-        x_copy(k, fs).start()
+    for way in range(2):
+        x_copy(way, fs).start()
     d_copy(0, fs, tp).start()
     loads[8].wait()
     loads[9].wait()
     z_step(KV, 1)
-
-    def relay(k):
-        x_copy(k, behind(k)).wait_recv()
-        d_copy(k, behind(k), tp).start()
-
-    for k in range(1, nf - 1):
-        relay(k)
+    z_step(QUERY, 1)
     for d in range(2, ns - 1):
         z_step(KV, d)
+    for way in range(2):
+        x_copy(way, beside[way]).wait_recv()
+        x_copy(way + 2, beside[way]).start()
+        d_copy(way + 1, beside[way], tp).start()
     own(OUT)
     spread(sp)
-    relay(nf - 1)
-    for d in range(1, ns - 1):
+    for d in range(2, ns - 1):
         z_step(QUERY, d)
     for j in (5, 6, 7, 10, 11, 12, 13, 14, 15):
         loads[j].wait()
     own(MIX)
+    for way in range(2, 4):
+        x_copy(way, beside[2]).wait_recv()
+    d_copy(3, beside[2], tp).start()
+    own(GATE)
     z_step(KV, ns - 1)
-    for k in range(nf):
-        d_copy(k, behind(k), 1 - tp).wait_recv()
+    for k, seq in enumerate((fs,) + beside):
+        d_copy(k, seq, 1 - tp).wait_recv()
 
     def tile(i):
         return pl.ds(pl.multiple_of(i * tokens, tokens), tokens)
@@ -400,27 +415,37 @@
 
         lax.fori_loop(0, nf, body, 0)
 
-    lane8 = lax.broadcasted_iota(jnp.int32, (tokens, wi.shape[1]), 1)
-    lane = lax.broadcasted_iota(jnp.int32, (tokens, 128), 1)
     row_at = lax.broadcasted_iota(jnp.int32, (tokens, tokens), 0)
     col_at = lax.broadcasted_iota(jnp.int32, (tokens, tokens), 1)
-    packed = jnp.zeros((tokens, 128), F32)
+    gates = jnp.concatenate([wi[...].astype(F32), wf[...].astype(F32)], axis=0).astype(BF16)
+    heads = wi.shape[0]
+    own_gate = lax.broadcasted_iota(jnp.int32, (2 * heads, tokens), 0)
+    own_bias = lax.broadcasted_iota(jnp.int32, (1, heads), 1)
+    bias_in = jnp.sum(jnp.where(own_bias == g, bias[0:1, :], 0.0), axis=1, keepdims=True)
+    bias_out = jnp.sum(jnp.where(own_bias == g, bias[1:2, :], 0.0), axis=1, keepdims=True)
+    line = lax.broadcasted_iota(jnp.int32, (128, tokens), 0)
+    packed = jnp.zeros((128, tokens), F32)
     for s in range(nf):
-        x = normed[s * tokens : (s + 1) * tokens, :]
-        entry = jnp.dot(x, wi[...], preferred_element_type=F32) + bias[0:1, :]
-        raw_forget = jnp.dot(x, wf[...], preferred_element_type=F32) + bias[1:2, :]
+        raw_gates = lax.dot_general(
+            gates,
+            normed[s * tokens : (s + 1) * tokens, :],
+            (((1,), (1,)), ((), ())),
+            preferred_element_type=F32,
+        )
+        entry = jnp.sum(jnp.where(own_gate == g, raw_gates, 0.0), axis=0, keepdims=True) + bias_in
         forget = (
-            jnp.minimum(raw_forget, 0.0) - jnp.log1p(jnp.exp(-jnp.abs(raw_forget))) + decay[s]
-        )
-        entry = jnp.sum(jnp.where(lane8 == g, entry, 0.0), axis=1, keepdims=True)
-        forget = jnp.sum(jnp.where(lane8 == g, forget, 0.0), axis=1, keepdims=True)
-        packed = jnp.where(lane == s, forget, packed)
-        packed = jnp.where(lane == nf + s, entry, packed)
-    ones = jnp.where(row_at >= col_at, 1.0, 0.0).astype(F32)
-    sums = jnp.dot(ones, packed, precision=HIGHEST_PRECISION, preferred_element_type=F32)
-    sums = jnp.where(lane < nf, sums, packed)
-    logs[...] = sums
-    logs_t[...] = sums.T
+            jnp.sum(jnp.where(own_gate == heads + g, raw_gates, 0.0), axis=0, keepdims=True)
+            + bias_out
+        )
+        shift = jnp.sum(jnp.where(own_gate[:heads] == g, decay[s], 0.0), axis=0, keepdims=True)
+        forget = jnp.minimum(forget, 0.0) - jnp.log1p(jnp.exp(-jnp.abs(forget))) + shift
+        packed = jnp.where(line == s, forget, packed)
+        packed = jnp.where(line == nf + s, entry, packed)
+    ones = jnp.where(row_at <= col_at, 1.0, 0.0).astype(F32)
+    sums = jnp.dot(packed, ones, precision=HIGHEST_PRECISION, preferred_element_type=F32)
+    sums = jnp.where(line < nf, sums, packed)
+    logs_t[...] = sums
+    logs[...] = sums.T
     project(KV, kv)
     for s in range(nf):
         rows = pl.ds(s * tokens, tokens)
@@ -434,7 +459,7 @@
         local_stat[s : s + 1, :] = jnp.broadcast_to(total, (1, 128))
         local_stat[nf + s : nf + s + 1, :] = jnp.broadcast_to(peak, (1, 128))
 
-    z_step(QUERY, ns - 1)
+    pass_on(sp)
     z_step(OUT, 1)
 
     def state_copies():
@@ -466,23 +491,29 @@
         for copy in state_copies():
             copy.start()
 
+    z_step(QUERY, ns - 1)
     for d in range(2, ns - 1):
         z_step(OUT, d)
-    own(GATE)
+    pass_step(1)
+    z_step(OUT, ns - 1)
+    z_step(MIX, 1)
+    for d in range(2, ns - 1):
+        pass_step(d)
+        z_step(MIX, d)
     project(QUERY, query)
 
     def mix_copy(m, k, seq, source):
         return remote(
             mine.at[m, seq],
             got.at[m, :, block(source, cols)],
-            m_send.at[m, k - 1],
-            m_recv.at[m, k - 1],
-            (sp, ahead(k), tp),
+            m_send.at[m, k],
+            m_recv.at[m, k],
+            (sp, beside[k], tp),
         )
 
     def hand_out(m):
-        for k in range(1, nf):
-            mix_copy(m, k, ahead(k), fs).start()
+        for k in (2, 0, 1):
+            mix_copy(m, k, beside[k], fs).start()
         got[m, :, block(fs, cols)] = mine[m, fs]
 
     scale = HEAD_DIM ** (-0.5)
@@ -510,11 +541,27 @@
         cell = cell * lax.rsqrt(jnp.mean(cell * cell, axis=-1, keepdims=True) + EPSILON)
         mine[1, s] = (cell * head_gain).astype(BF16)
 
-    for d in range(1, ns - 1):
-        z_step(MIX, d)
     hand_out(1)
-    z_step(OUT, ns - 1)
+    gate_first, gate_count = SPANS[GATE]
+
+    def gate_part(owner, first=False):
+        def body(i, carried):
+            part = jnp.dot(
+                normed[tile(i), block(owner, depth)],
+                wbuf[block(owner, depth), gate_first * cols : (gate_first + gate_count) * cols],
+                preferred_element_type=F32,
+            )
+            gate_sum[tile(i), :] = part if first else gate_sum[tile(i), :] + part
+            return carried
+
+        lax.fori_loop(0, nf, body, 0)
+
+    gate_part(sp, True)
+    z_step(GATE, 1, gate_part)
+    pass_step(ns - 1)
     z_step(MIX, ns - 1)
+    for d in range(2, ns - 1):
+        z_step(GATE, d, gate_part)
 
     def rim_copy():
         return remote(
@@ -545,24 +592,6 @@
     def _():
         rim_copy().start()
 
-    gate_first, gate_count = SPANS[GATE]
-
-    def gate_part(owner, first=False):
-        def body(i, carried):
-            part = jnp.dot(
-                normed[tile(i), block(owner, depth)],
-                wbuf[block(owner, depth), gate_first * cols : (gate_first + gate_count) * cols],
-                preferred_element_type=F32,
-            )
-            gate_sum[tile(i), :] = part if first else gate_sum[tile(i), :] + part
-            return carried
-
-        lax.fori_loop(0, nf, body, 0)
-
-    gate_part(sp, True)
-    for d in range(1, ns - 1):
-        z_step(GATE, d, gate_part)
-
     @pl.when(has_down)
     def _():
         rim_copy().wait_recv()
@@ -576,13 +605,13 @@
         mixed[s * tokens : (s + 1) * tokens, :] = total
 
     def arrived(owner, carried):
-        for k in range(1, nf):
-            p_copy(owner, k, behind(k)).wait_recv()
+        for way in range(2, 4):
+            p_copy(owner, way, beside[2]).wait_recv()
         return carried
 
     lax.fori_loop(0, ns, arrived, 0)
-    for k in range(1, nf):
-        mix_copy(1, k, ahead(k), behind(k)).wait_recv()
+    for k in range(nf - 1):
+        mix_copy(1, k, beside[k], beside[k]).wait_recv()
 
     def memory_share(i, carried):
         acc[:, block(i, ocols)] = jnp.dot(
@@ -592,13 +621,30 @@
 
     lax.fori_loop(0, ns, memory_share, 0)
 
-    z_step(GATE, ns - 1, gate_part)
-    for s in range(nf):
-        rows = slice(s * tokens, (s + 1) * tokens)
-        mine[0, s] = (gate_sum[rows, :].astype(BF16).astype(F32) * mixed[rows, :]).astype(BF16)
-    hand_out(0)
-    for k in range(1, nf):
-        mix_copy(0, k, ahead(k), behind(k)).wait_recv()
+    z_step(GATE, ns - 1)
+    at_end = jnp.logical_not(has_up & has_down)
+    farthest = lax.rem(sp + ns - 1, 2 * (ns - 1))
+
+    def convolve(seq):
+        @pl.when(at_end)
+        def _():
+            gate_sum[tile(seq), :] = gate_sum[tile(seq), :] + jnp.dot(
+                normed[tile(seq), block(farthest, depth)],
+                wbuf[
+                    block(farthest, depth), gate_first * cols : (gate_first + gate_count) * cols
+                ],
+                preferred_element_type=F32,
+            )
+
+        return (gate_sum[tile(seq), :].astype(BF16).astype(F32) * mixed[tile(seq), :]).astype(BF16)
+
+    order = (2, 0, 1)
+    for step, k in enumerate(order):
+        mine[0, beside[k]] = convolve(beside[k])
+        if step > 0:
+            mix_copy(0, order[step - 1], beside[order[step - 1]], fs).start()
+    got[0, :, block(fs, cols)] = convolve(fs)
+    mix_copy(0, order[-1], beside[order[-1]], fs).start()
 
     def e_copy(i):
         return remote(
@@ -609,14 +655,23 @@
             partner,
         )
 
-    def finish(i, carried):
+    def add_pair(i, pair):
         acc[:, block(i, ocols)] = acc[:, block(i, ocols)] + jnp.dot(
-            got[0], wo[0, :, block(i, ocols)], preferred_element_type=F32
-        )
-        e_copy(i).start()
-        return carried
-
-    lax.fori_loop(0, ns, finish, 0)
+            got[0, :, block(pair, 2 * cols)],
+            wo[0, block(pair, 2 * cols), block(i, ocols)],
+            preferred_element_type=F32,
+        )
+
+    mix_copy(0, 0, beside[0], beside[0]).wait_recv()
+    for i in range(ns):
+        add_pair(i, fy)
+    for k in (1, 2):
+        mix_copy(0, k, beside[k], beside[k]).wait_recv()
+    for i in range(ns):
+        add_pair(i, 1 - fy)
+        if i > 0:
+            e_copy(i - 1).start()
+    e_copy(ns - 1).start()
 
     def merge(i, carried):
         e_copy(i).wait_recv()
@@ -629,17 +684,18 @@
 
     def sent(i, carried):
         e_copy(i).wait_send()
-        for k in range(1, nf):
-            p_copy(i, k, fs).wait_send()
+        for way in range(4):
+            p_copy(i, way, (fs, fs, beside[0], beside[1])[way]).wait_send()
         return carried
 
     lax.fori_loop(0, ns, sent, 0)
-    for k in range(1, nf):
-        x_copy(k, fs).wait_send()
-        d_copy(k, behind(k), tp).wait_send()
+    for way in range(4):
+        x_copy(way, (fs, fs, beside[0], beside[1])[way]).wait_send()
+    for k, seq in enumerate((fs,) + beside):
+        d_copy(k, seq, tp).wait_send()
+    for k in range(nf - 1):
         for m in range(2):
-            mix_copy(m, k, ahead(k), fs).wait_send()
-    d_copy(0, fs, tp).wait_send()
+            mix_copy(m, k, beside[k], fs).wait_send()
     for side in range(2):
         for d in range(ns - 1):
 
@@ -667,7 +723,7 @@
     vmem = pltpu.VMEM
     return pl.pallas_call(
         functools.partial(layer_kernel, ns, nf),
-        out_shape=jax.ShapeDtypeStruct((half, ns * ocols), BF16),
+        out_shape=pltpu.VMEM((half, ns * ocols), BF16),
         in_specs=[anywhere] * 16,
         out_specs=pl.BlockSpec(memory_space=pltpu.VMEM),
         scratch_shapes=[
@@ -700,14 +756,14 @@
             vmem((tokens, ns * ocols), F32),
             vmem((half, ns * ocols), F32),
             dma((16,)),
-            dma((nf - 1,)),
-            dma((nf - 1,)),
+            dma((4,)),
+            dma((4,)),
             dma((nf,)),
             dma((nf,)),
             dma((2, ns - 1, PARTS)),
             dma((2, ns - 1, PARTS)),
-            dma((ns, nf - 1)),
-            dma((ns, nf - 1)),
+            dma((ns, 4)),
+            dma((ns, 4)),
             dma((2,)),
             dma((2,)),
             dma,
@@ -718,7 +774,7 @@
             dma((ns,)),
         ],
         compiler_params=pltpu.CompilerParams(
-            collective_id=0, has_side_effects=True, vmem_limit_bytes=63 * 1024 * 1024
+            collective_id=0, has_side_effects=True, vmem_limit_bytes=54 * 1024 * 1024
         ),
     )(act, gain, *weights, wi, wf, bias, decay, taps, head, w_out_conv, w_out_mem)
 
@@ -745,15 +801,15 @@
     heads_here = MEMORY_HEADS // (lax.axis_size("fs") * lax.axis_size("tp"))
     channels = w_conv_gate.shape[1]
     ns, nf, nt = (lax.axis_size("sp"), lax.axis_size("fs"), lax.axis_size("tp"))
-    if 2 <= ns <= 8 and nf % 2 == 0 and nt == 2 and heads_here == 1 and channels == HEAD_DIM:
+    if 2 <= ns <= 8 and nf == 4 and nt == 2 and heads_here == 1 and channels == HEAD_DIM:
         return whole_layer(
             activations[0],
             norm_gain[None, :],
             (w_key, w_value, w_query, w_conv_mult, w_conv_in, w_conv_gate),
-            w_input_gate,
-            w_forget_gate,
+            w_input_gate.T,
+            w_forget_gate.T,
             gate_bias,
-            decay_shift,
+            decay_shift.transpose(0, 2, 1),
             conv_taps,
             head_gain[None, :],
             w_out_conv,

time: 98 us -> 86.3 us (0.88)
  Pallas kernels: 92.1 us -> 85.3 us
  local copies, waits for them, and re-layouts: 5.64 us -> 0.8 us
    pallas_call x1, Pallas kernels: 92.1 us -> 85.3 us  [whole_layer(): pl.pallas_call(functools.partial(layer_kernel, ns, nf), out_shape=pltpu.V...]
    unnamed x8 -> x1, local copies, waits for them, and re-layouts: 5.64 us -> 0.8 us
where the time goes in v2:
time: 86.3 us; the launch traced here: 86.1 us
  Pallas kernels  85.3 us (99%)
    pallas_call x1, Pallas kernels, whole_layer(): pl.pallas_call(functools.partial(layer_kernel, ns, nf), out_shape=pltpu.V...  85.3 us

profile of v2, /device:TPU:25, one launch (start us, length us, event | category | flops | bytes accessed | tf_op | source)
XLA Modules:
  0.0 86.1 jit_solution(17091724344655785976)
XLA Ops:
  0.0 85.3 %shard_map.154 = bf16[128,2048]{1,0:T(8,128)(2,1)S(1)} custom-call(bf16[256,2048]{1,0:T(8,128)(2,1)} %bitcast.8, f32[1,2048]{1,0:T(1,128)} %bitcast.12, bf16[512,128]{1,0:T(8,128)(2,1)} %w0_ref.1, bf16[512,128]{1,0:T(8,128)(2,1)} %w1_ref.1, bf16[512,128]{1,0:T(8,128)(2,1)} %w2_ref.1, bf16[512,128]{1,0:T(8,128)(2,1)} %w3_ref.1, bf16[512,128]{1,0:T(8,128)(2,1)} %w4_ref.1, ...), custom_call_target="tpu_custom_call" | custom-call | tf_op jit(solution)/shard_map/pallas_call | solution.py:724
  85.3 0.8 copy.18

commit v3 on v2

--- a/solution.py
+++ b/solution.py
@@ -176,17 +176,19 @@
     query,
     logs,
     logs_t,
-    local_state,
     local_stat,
+    passed,
+    states,
+    stats,
     carry,
     carry_m,
-    passed,
-    passed_m,
     padded,
-    mixed,
-    gate_sum,
+    gated,
     mine,
     got,
+    guest,
+    guest_padded,
+    guest_mine,
     acc,
     other,
     load_sem,
@@ -206,6 +208,14 @@
     m_recv,
     e_send,
     e_recv,
+    t_send,
+    t_recv,
+    u_send,
+    u_recv,
+    v_send,
+    v_recv,
+    c_send,
+    c_recv,
 ):
     sp, fs, tp = (lax.axis_index("sp"), lax.axis_index("fs"), lax.axis_index("tp"))
     g = fs * 2 + tp
@@ -219,6 +229,11 @@
     fy, fx = (fs // 2, lax.rem(fs, 2))
     beside = (fy * 2 + 1 - fx, (1 - fy) * 2 + fx, (1 - fy) * 2 + 1 - fx)
 
+    pair = sp + 1 - 2 * lax.rem(sp, 2)
+    hosts = has_up & has_down
+    guests = jnp.logical_not(hosts)
+    around = (fs,) + beside
+
     def block(index, size):
         return pl.ds(pl.multiple_of(index * size, size), size)
 
@@ -257,15 +272,11 @@
     barrier = pltpu.get_barrier_semaphore()
     for peer in beside:
         pl.semaphore_signal(barrier, inc=1, device_id=(sp, peer, tp), device_id_type=MESH)
+        pl.semaphore_signal(barrier, inc=1, device_id=(pair, peer, tp), device_id_type=MESH)
+    for off in range(1, ns):
+        there = (lax.rem(sp + off, ns), fs, tp)
+        pl.semaphore_signal(barrier, inc=1, device_id=there, device_id_type=MESH)
     pl.semaphore_signal(barrier, inc=1, device_id=partner, device_id_type=MESH)
-
-    @pl.when(has_up)
-    def _():
-        pl.semaphore_signal(barrier, inc=1, device_id=up, device_id_type=MESH)
-
-    @pl.when(has_down)
-    def _():
-        pl.semaphore_signal(barrier, inc=1, device_id=down, device_id_type=MESH)
 
     def place(part, owner):
         if part == OUT:
@@ -286,14 +297,18 @@
     def owner_of(side, d):
         return sp - d if side == 0 else sp + d
 
-    def arrives(side, d):
-        return (sp - d >= 0) if side == 0 else (sp + d < ns)
-
-    def sends(side, d):
-        return arrives(side, d) & (has_up if side == 0 else has_down)
+    def arrives(part, side, d):
+        there = (sp - d >= 0) if side == 0 else (sp + d < ns)
+        return there & hosts if part in (MIX, GATE) else there
+
+    def sends(part, side, d):
+        there = (sp - d >= 0) if side == 0 else (sp + d < ns)
+        if part in (MIX, GATE):
+            return there & ((sp + 2 < ns) if side == 0 else (sp > 1))
+        return there & (has_up if side == 0 else has_down)
 
     def z_send(part, side, d):
-        @pl.when(sends(side, d))
+        @pl.when(sends(part, side, d))
         def _():
             z_copy(part, side, d, owner_of(side, d)).start()
 
@@ -302,14 +317,13 @@
             z_send(part, side, 0)
 
     def p_copy(owner, way, row):
-        span = ((0, 2), (0, 2), (0, 1), (1, 1))[way]
-        there = wo.at[pl.ds(*span), block(row, cols), block(owner, ocols)]
+        there = wo.at[:, block(row, cols), block(owner, ocols)]
         return remote(
             there,
             there,
             p_send.at[owner, way],
             p_recv.at[owner, way],
-            (sp, beside[(0, 1, 1, 0)[way]], tp),
+            (sp, beside[(0, 1, 0)[way]], tp),
         )
 
     def spread(owner):
@@ -317,21 +331,20 @@
             p_copy(owner, way, fs).start()
 
     def pass_on(owner):
-        for way in range(2):
-            p_copy(owner, way, beside[way]).wait_recv()
-            p_copy(owner, way + 2, beside[way]).start()
+        p_copy(owner, 1, beside[1]).wait_recv()
+        p_copy(owner, 2, beside[1]).start()
 
     def pass_step(d):
         for side in range(2):
 
-            @pl.when(arrives(side, d))
+            @pl.when(arrives(OUT, side, d))
             def _():
                 pass_on(owner_of(side, d))
 
-    def z_step(part, d, use=None):
+    def z_step(part, d):
         for side in range(2):
 
-            @pl.when(arrives(side, d))
+            @pl.when(arrives(part, side, d))
             def _():
                 owner = owner_of(side, d)
                 z_copy(part, side, d - 1, owner).wait_recv()
@@ -339,8 +352,6 @@
                     z_send(part, side, d)
                 if part == OUT:
                     spread(owner)
-                if use is not None:
-                    use(owner)
 
     def x_copy(way, seq):
         first, rows = ((0, half), (0, half), (0, half // 2), (half // 2, half // 2))[way]
@@ -353,51 +364,48 @@
         there = normed.at[pl.ds(pl.multiple_of(seq * tokens + part * half, half), half)]
         return remote(there, there, d_send.at[k], d_recv.at[k], partner)
 
-    loads[2].wait()
-    loads[3].wait()
-    pl.semaphore_wait(barrier, nf + has_up.astype(jnp.int32) + has_down.astype(jnp.int32))
-    own(KV)
-    loads[0].wait()
-    loads[1].wait()
-    step = 32
-
-    def norm_rows(i, carried):
-        x = raw[pl.ds(pl.multiple_of(i * step, step), step), :].astype(F32)
-        scale = lax.rsqrt(jnp.mean(x * x, axis=-1, keepdims=True) + EPSILON)
-        rows = pl.ds(pl.multiple_of(fs * tokens + tp * half + i * step, step), step)
-        normed[rows, :] = (x * scale * gain[...]).astype(BF16)
-        return carried
-
-    lax.fori_loop(0, half // step, norm_rows, 0)
-    loads[4].wait()
-    own(QUERY)
-    for way in range(2):
-        x_copy(way, fs).start()
-    d_copy(0, fs, tp).start()
-    loads[8].wait()
-    loads[9].wait()
-    z_step(KV, 1)
-    z_step(QUERY, 1)
-    for d in range(2, ns - 1):
-        z_step(KV, d)
-    for way in range(2):
+    def guest_rows(ref, seq, part):
+        return ref.at[pl.ds(pl.multiple_of(seq * tokens + part * half, half), half)]
+
+    def t_copy(j):
+        return remote(
+            guest_rows(normed, around[j], tp),
+            guest_rows(guest, around[j], tp),
+            t_send.at[j],
+            t_recv.at[j],
+            (pair, fs, tp),
+        )
+
+    def u_copy(j, seq):
+        there = guest_rows(guest, seq, tp)
+        return remote(there, there, u_send.at[j], u_recv.at[j], (sp, beside[1], tp))
+
+    def v_copy(k, part):
+        there = guest_rows(guest, around[k], part)
+        return remote(there, there, v_send.at[k], v_recv.at[k], partner)
+
+    def guest_from_pair(j):
+        @pl.when(hosts)
+        def _():
+            t_copy(j).wait_recv()
+            u_copy(j, around[j]).start()
+            v_copy(j, tp).start()
+
+    def guest_from_beside(j):
+        @pl.when(hosts)
+        def _():
+            u_copy(j, around[2 + j]).wait_recv()
+            v_copy(2 + j, tp).start()
+
+    def guest_to_pair(j):
+        @pl.when(guests)
+        def _():
+            t_copy(j).start()
+
+    def activations_in(way):
         x_copy(way, beside[way]).wait_recv()
         x_copy(way + 2, beside[way]).start()
         d_copy(way + 1, beside[way], tp).start()
-    own(OUT)
-    spread(sp)
-    for d in range(2, ns - 1):
-        z_step(QUERY, d)
-    for j in (5, 6, 7, 10, 11, 12, 13, 14, 15):
-        loads[j].wait()
-    own(MIX)
-    for way in range(2, 4):
-        x_copy(way, beside[2]).wait_recv()
-    d_copy(3, beside[2], tp).start()
-    own(GATE)
-    z_step(KV, ns - 1)
-    for k, seq in enumerate((fs,) + beside):
-        d_copy(k, seq, 1 - tp).wait_recv()
 
     def tile(i):
         return pl.ds(pl.multiple_of(i * tokens, tokens), tokens)
@@ -414,6 +422,180 @@
             return carried
 
         lax.fori_loop(0, nf, body, 0)
+
+    def mix_copy(m, k, seq, source):
+        return remote(
+            mine.at[m, seq],
+            got.at[m, :, block(source, cols)],
+            m_send.at[m, k],
+            m_recv.at[m, k],
+            (sp, beside[k], tp),
+        )
+
+    def hand_out(m):
+        for k in (2, 0, 1):
+            mix_copy(m, k, beside[k], fs).start()
+        got[m, :, block(fs, cols)] = mine[m, fs]
+
+    def state_copies(off, source):
+        to = (lax.rem(sp + off, ns), fs, tp)
+        return (
+            remote(
+                local_stat, stats.at[source], s_send.at[0, off - 1], s_recv.at[0, off - 1], to
+            ),
+            remote(passed, states.at[source], s_send.at[1, off - 1], s_recv.at[1, off - 1], to),
+        )
+
+    def states_out():
+        for off in range(ns - 1, 0, -1):
+
+            @pl.when(sp + off < ns)
+            def _():
+                for copy in state_copies(off, sp):
+                    copy.start()
+
+    def states_in():
+        for off in range(1, ns):
+
+            @pl.when(sp - off >= 0)
+            def _():
+                for copy in state_copies(off, sp - off):
+                    copy.wait_recv()
+
+        carry[...] = jnp.zeros_like(carry)
+        carry_m[...] = jnp.zeros_like(carry_m)
+        for source in range(ns - 1):
+
+            @pl.when(source < sp)
+            def _():
+                for s in range(nf):
+                    before = stats[source, s : s + 1, :] + carry_m[s : s + 1, :]
+                    peak = stats[source, nf + s : nf + s + 1, :]
+                    top = jnp.maximum(before, peak)
+                    carry[s] = jnp.exp(before - top) * carry[s] + jnp.exp(peak - top) * states[
+                        source, s
+                    ].astype(F32)
+                    carry_m[s : s + 1, :] = top
+
+    def rim_copy():
+        return remote(
+            padded.at[:, pl.ds(tokens, RIM), :],
+            padded.at[:, pl.ds(0, RIM), :],
+            r_send,
+            r_recv,
+            up,
+        )
+
+    inner = hosts & (sp + 2 < ns)
+    outer = hosts & (sp > 1)
+
+    def products(source, seq, held):
+        three = jnp.dot(
+            source[tile(seq), :],
+            wbuf[:, SPANS[MIX][0] * cols :],
+            preferred_element_type=F32,
+        ).astype(BF16)
+        both = three[:, : 2 * cols].astype(F32)
+        held[seq, RIM:, :] = (both[:, :cols] * both[:, cols:]).astype(BF16).astype(F32)
+        return three[:, 2 * cols :]
+
+    def convolve(held, seq, gate):
+        tap = taps[:, block(g, cols)]
+        total = jnp.zeros((tokens, cols), F32)
+        for j in range(TAPS):
+            at = RIM - (TAPS - 1) + j
+            total = total + tap[j : j + 1, :] * held[seq, at : at + tokens, :]
+        return (gate.astype(F32) * total).astype(BF16)
+
+    def c_copy(k, seq, source):
+        return remote(
+            guest_mine.at[seq],
+            got.at[0, :, block(source, cols)],
+            c_send.at[k],
+            c_recv.at[k],
+            (pair, around[k], tp),
+        )
+
+    def own_products():
+        @pl.when(hosts)
+        def _():
+            def body(i, carried):
+                gated[tile(i), :] = products(normed, i, padded)
+                return carried
+
+            lax.fori_loop(0, nf, body, 0)
+
+        @pl.when(inner)
+        def _():
+            rim_copy().start()
+
+    def guest_part(k):
+        seq = around[k]
+        v_copy(k, 1 - tp).wait_recv()
+        gate = products(guest, seq, guest_padded)
+        guest_padded[seq, 0:RIM, :] = jnp.where(inner, 0.0, padded[seq, tokens : tokens + RIM, :])
+        guest_mine[seq] = convolve(guest_padded, seq, gate)
+
+    def own_part(seq):
+        @pl.when(inner)
+        def _():
+            padded[seq, 0:RIM, :] = guest_padded[seq, tokens : tokens + RIM, :]
+
+        return convolve(padded, seq, gated[tile(seq), :])
+
+    loads[2].wait()
+    loads[3].wait()
+    pl.semaphore_wait(barrier, 2 * (nf - 1) + ns)
+    own(KV)
+    loads[8].wait()
+    loads[9].wait()
+    own(OUT)
+    spread(sp)
+    loads[0].wait()
+    loads[1].wait()
+    step = 32
+
+    def norm_rows(i, carried):
+        x = raw[pl.ds(pl.multiple_of(i * step, step), step), :].astype(F32)
+        scale = lax.rsqrt(jnp.mean(x * x, axis=-1, keepdims=True) + EPSILON)
+        rows = pl.ds(pl.multiple_of(fs * tokens + tp * half + i * step, step), step)
+        normed[rows, :] = (x * scale * gain[...]).astype(BF16)
+        return carried
+
+    lax.fori_loop(0, half // step, norm_rows, 0)
+    loads[4].wait()
+    own(QUERY)
+    for j in (5, 6, 7):
+        loads[j].wait()
+    own(GATE)
+    for way in range(2):
+        x_copy(way, fs).start()
+    d_copy(0, fs, tp).start()
+    z_step(OUT, 1)
+    z_step(KV, 1)
+    guest_to_pair(0)
+    for way in range(2):
+        activations_in(way)
+    pass_on(sp)
+    z_step(QUERY, 1)
+    z_step(OUT, 2)
+    own(MIX)
+    z_step(KV, 2)
+    z_step(QUERY, 2)
+    guest_to_pair(1)
+    pass_step(1)
+    z_step(MIX, 1)
+    for way in range(2, 4):
+        x_copy(way, beside[2]).wait_recv()
+    d_copy(3, beside[2], tp).start()
+    z_step(OUT, 3)
+    z_step(KV, 3)
+    z_step(GATE, 1)
+    guest_from_pair(0)
+    for j in range(10, 16):
+        loads[j].wait()
+    for k, seq in enumerate(around):
+        d_copy(k, seq, 1 - tp).wait_recv()
 
     row_at = lax.broadcasted_iota(jnp.int32, (tokens, tokens), 0)
     col_at = lax.broadcasted_iota(jnp.int32, (tokens, tokens), 1)
@@ -453,68 +635,31 @@
         reach = total - logs[:, s : s + 1] + logs[:, nf + s : nf + s + 1]
         peak = jnp.max(reach, axis=0, keepdims=True)
         weighted = (kv[rows, cols:].astype(F32) * jnp.exp(reach - peak)).astype(BF16)
-        local_state[s] = lax.dot_general(
+        passed[s] = lax.dot_general(
             kv[rows, :cols], weighted, (((0,), (0,)), ((), ())), preferred_element_type=F32
-        )
+        ).astype(BF16)
         local_stat[s : s + 1, :] = jnp.broadcast_to(total, (1, 128))
         local_stat[nf + s : nf + s + 1, :] = jnp.broadcast_to(peak, (1, 128))
 
-    pass_on(sp)
-    z_step(OUT, 1)
-
-    def state_copies():
-        return (
-            remote(passed_m, carry_m, s_send.at[0], s_recv.at[0], up),
-            remote(passed, carry, s_send.at[1], s_recv.at[1], up),
-        )
-
-    @pl.when(jnp.logical_not(has_down))
+    z_step(QUERY, 3)
+    z_step(GATE, 2)
+    states_out()
+    pass_step(2)
+    guest_from_pair(1)
+    pass_step(3)
+    guest_from_beside(0)
+    z_step(MIX, 2)
+    own_products()
+
+    @pl.when(hosts)
     def _():
-        carry[...] = jnp.zeros_like(carry)
-        carry_m[...] = jnp.zeros_like(carry_m)
-
-    @pl.when(has_down)
-    def _():
-        for copy in state_copies():
-            copy.wait_recv()
-
-    @pl.when(has_up)
-    def _():
-        for s in range(nf):
-            before = local_stat[s : s + 1, :] + carry_m[s : s + 1, :]
-            peak = local_stat[nf + s : nf + s + 1, :]
-            top = jnp.maximum(before, peak)
-            passed[s] = (
-                jnp.exp(before - top) * carry[s].astype(F32) + jnp.exp(peak - top) * local_state[s]
-            ).astype(BF16)
-            passed_m[s : s + 1, :] = top
-        for copy in state_copies():
-            copy.start()
-
-    z_step(QUERY, ns - 1)
-    for d in range(2, ns - 1):
-        z_step(OUT, d)
-    pass_step(1)
-    z_step(OUT, ns - 1)
-    z_step(MIX, 1)
-    for d in range(2, ns - 1):
-        pass_step(d)
-        z_step(MIX, d)
+        for k in range(nf - 1):
+            guest_part(k)
+            if k > 0:
+                c_copy(k - 1, around[k - 1], fs).start()
+
+    states_in()
     project(QUERY, query)
-
-    def mix_copy(m, k, seq, source):
-        return remote(
-            mine.at[m, seq],
-            got.at[m, :, block(source, cols)],
-            m_send.at[m, k],
-            m_recv.at[m, k],
-            (sp, beside[k], tp),
-        )
-
-    def hand_out(m):
-        for k in (2, 0, 1):
-            mix_copy(m, k, beside[k], fs).start()
-        got[m, :, block(fs, cols)] = mine[m, fs]
 
     scale = HEAD_DIM ** (-0.5)
     head_gain = head[:, block(g, cols)]
@@ -535,78 +680,39 @@
         weights = (jnp.exp(pairs - top) * scores).astype(BF16)
         cell = jnp.dot(weights, kv[rows, cols:], preferred_element_type=F32)
         cell = cell + jnp.exp(carried - top) * jnp.dot(
-            query[rows, :], carry[s], preferred_element_type=F32
+            query[rows, :], carry[s].astype(BF16), preferred_element_type=F32
         )
         cell = cell * scale
         cell = cell * lax.rsqrt(jnp.mean(cell * cell, axis=-1, keepdims=True) + EPSILON)
         mine[1, s] = (cell * head_gain).astype(BF16)
 
     hand_out(1)
-    gate_first, gate_count = SPANS[GATE]
-
-    def gate_part(owner, first=False):
-        def body(i, carried):
-            part = jnp.dot(
-                normed[tile(i), block(owner, depth)],
-                wbuf[block(owner, depth), gate_first * cols : (gate_first + gate_count) * cols],
-                preferred_element_type=F32,
-            )
-            gate_sum[tile(i), :] = part if first else gate_sum[tile(i), :] + part
-            return carried
-
-        lax.fori_loop(0, nf, body, 0)
-
-    gate_part(sp, True)
-    z_step(GATE, 1, gate_part)
-    pass_step(ns - 1)
-    z_step(MIX, ns - 1)
-    for d in range(2, ns - 1):
-        z_step(GATE, d, gate_part)
-
-    def rim_copy():
-        return remote(
-            padded.at[:, pl.ds(tokens, RIM), :],
-            padded.at[:, pl.ds(0, RIM), :],
-            r_send,
-            r_recv,
-            up,
-        )
-
-    def product(i, carried):
-        both = jnp.dot(
-            normed[tile(i), :],
-            wbuf[:, SPANS[MIX][0] * cols : SPANS[GATE][0] * cols],
-            preferred_element_type=F32,
-        ).astype(BF16)
-        both = both.astype(F32)
-        padded[i, RIM:, :] = (both[:, :cols] * both[:, cols:]).astype(BF16).astype(F32)
-        return carried
-
-    lax.fori_loop(0, nf, product, 0)
-
-    @pl.when(jnp.logical_not(has_down))
-    def _():
-        padded[:, 0:RIM, :] = jnp.zeros((nf, RIM, cols), F32)
-
-    @pl.when(has_up)
-    def _():
-        rim_copy().start()
-
-    @pl.when(has_down)
+
+    @pl.when(outer)
     def _():
         rim_copy().wait_recv()
 
-    tap = taps[:, block(g, cols)]
-    for s in range(nf):
-        total = jnp.zeros((tokens, cols), F32)
-        for j in range(TAPS):
-            at = RIM - (TAPS - 1) + j
-            total = total + tap[j : j + 1, :] * padded[s, at : at + tokens, :]
-        mixed[s * tokens : (s + 1) * tokens, :] = total
+    @pl.when(hosts)
+    def _():
+        c_copy(nf - 2, around[nf - 2], fs).start()
+        mine[0, beside[0]] = own_part(beside[0])
+        mine[0, beside[1]] = own_part(beside[1])
+        mix_copy(0, 0, beside[0], fs).start()
+        got[0, :, block(fs, cols)] = own_part(fs)
+        mix_copy(0, 1, beside[1], fs).start()
+
+    guest_from_beside(1)
+
+    @pl.when(hosts)
+    def _():
+        guest_part(nf - 1)
+        mine[0, beside[2]] = own_part(beside[2])
+        c_copy(nf - 1, around[nf - 1], fs).start()
+        mix_copy(0, 2, beside[2], fs).start()
 
     def arrived(owner, carried):
-        for way in range(2, 4):
-            p_copy(owner, way, beside[2]).wait_recv()
+        p_copy(owner, 0, beside[0]).wait_recv()
+        p_copy(owner, 2, beside[2]).wait_recv()
         return carried
 
     lax.fori_loop(0, ns, arrived, 0)
@@ -620,31 +726,6 @@
         return carried
 
     lax.fori_loop(0, ns, memory_share, 0)
-
-    z_step(GATE, ns - 1)
-    at_end = jnp.logical_not(has_up & has_down)
-    farthest = lax.rem(sp + ns - 1, 2 * (ns - 1))
-
-    def convolve(seq):
-        @pl.when(at_end)
-        def _():
-            gate_sum[tile(seq), :] = gate_sum[tile(seq), :] + jnp.dot(
-                normed[tile(seq), block(farthest, depth)],
-                wbuf[
-                    block(farthest, depth), gate_first * cols : (gate_first + gate_count) * cols
-                ],
-                preferred_element_type=F32,
-            )
-
-        return (gate_sum[tile(seq), :].astype(BF16).astype(F32) * mixed[tile(seq), :]).astype(BF16)
-
-    order = (2, 0, 1)
-    for step, k in enumerate(order):
-        mine[0, beside[k]] = convolve(beside[k])
-        if step > 0:
-            mix_copy(0, order[step - 1], beside[order[step - 1]], fs).start()
-    got[0, :, block(fs, cols)] = convolve(fs)
-    mix_copy(0, order[-1], beside[order[-1]], fs).start()
 
     def e_copy(i):
         return remote(
@@ -662,11 +743,28 @@
             preferred_element_type=F32,
         )
 
-    mix_copy(0, 0, beside[0], beside[0]).wait_recv()
+    @pl.when(hosts)
+    def _():
+        mix_copy(0, 0, beside[0], beside[0]).wait_recv()
+
+    @pl.when(guests)
+    def _():
+        for k in range(2):
+            c_copy(k, around[k], around[k]).wait_recv()
+
     for i in range(ns):
         add_pair(i, fy)
-    for k in (1, 2):
-        mix_copy(0, k, beside[k], beside[k]).wait_recv()
+
+    @pl.when(hosts)
+    def _():
+        for k in (1, 2):
+            mix_copy(0, k, beside[k], beside[k]).wait_recv()
+
+    @pl.when(guests)
+    def _():
+        for k in range(2, nf):
+            c_copy(k, around[k], around[k]).wait_recv()
+
     for i in range(ns):
         add_pair(i, 1 - fy)
         if i > 0:
@@ -684,31 +782,52 @@
 
     def sent(i, carried):
         e_copy(i).wait_send()
-        for way in range(4):
-            p_copy(i, way, (fs, fs, beside[0], beside[1])[way]).wait_send()
+        for way in range(3):
+            p_copy(i, way, (fs, fs, beside[1])[way]).wait_send()
         return carried
 
     lax.fori_loop(0, ns, sent, 0)
     for way in range(4):
         x_copy(way, (fs, fs, beside[0], beside[1])[way]).wait_send()
-    for k, seq in enumerate((fs,) + beside):
+    for k, seq in enumerate(around):
         d_copy(k, seq, tp).wait_send()
     for k in range(nf - 1):
-        for m in range(2):
-            mix_copy(m, k, beside[k], fs).wait_send()
+        mix_copy(1, k, beside[k], fs).wait_send()
+
+    @pl.when(hosts)
+    def _():
+        for k in range(nf - 1):
+            mix_copy(0, k, beside[k], fs).wait_send()
+        for k in range(nf):
+            v_copy(k, tp).wait_send()
+            c_copy(k, around[k], fs).wait_send()
+        for j in range(2):
+            u_copy(j, around[j]).wait_send()
+
+    @pl.when(guests)
+    def _():
+        for j in range(2):
+            t_copy(j).wait_send()
+
+    @pl.when(inner)
+    def _():
+        rim_copy().wait_send()
+
     for side in range(2):
         for d in range(ns - 1):
-
-            @pl.when(sends(side, d))
-            def _():
-                for part in range(PARTS):
-                    z_copy(part, side, d, owner_of(side, d)).wait_send()
-
-    @pl.when(has_up)
-    def _():
-        for copy in state_copies():
-            copy.wait_send()
-        rim_copy().wait_send()
+            for parts in ((KV, QUERY, OUT), (MIX, GATE)):
+
+                @pl.when(sends(parts[0], side, d))
+                def _():
+                    for part in parts:
+                        z_copy(part, side, d, owner_of(side, d)).wait_send()
+
+    for off in range(1, ns):
+
+        @pl.when(sp + off < ns)
+        def _():
+            for copy in state_copies(off, sp):
+                copy.wait_send()
 
 
 def whole_layer(act, gain, weights, wi, wf, bias, decay, taps, head, w_out_conv, w_out_mem):
@@ -742,17 +861,19 @@
             vmem((count, cols), BF16),
             vmem((tokens, 128), F32),
             vmem((128, tokens), F32),
-            vmem((nf, cols, cols), F32),
             vmem((2 * nf, 128), F32),
             vmem((nf, cols, cols), BF16),
-            vmem((8, 128), F32),
-            vmem((nf, cols, cols), BF16),
-            vmem((8, 128), F32),
+            vmem((ns - 1, nf, cols, cols), BF16),
+            vmem((ns - 1, 2 * nf, 128), F32),
+            vmem((nf, cols, cols), F32),
+            vmem((nf, 128), F32),
             vmem((nf, RIM + tokens, cols), F32),
-            vmem((count, cols), F32),
-            vmem((count, cols), F32),
+            vmem((count, cols), BF16),
             vmem((2, nf, tokens, cols), BF16),
             vmem((2, tokens, nf * cols), BF16),
+            vmem((count, model), BF16),
+            vmem((nf, RIM + tokens, cols), F32),
+            vmem((nf, tokens, cols), BF16),
             vmem((tokens, ns * ocols), F32),
             vmem((half, ns * ocols), F32),
             dma((16,)),
@@ -762,16 +883,24 @@
             dma((nf,)),
             dma((2, ns - 1, PARTS)),
             dma((2, ns - 1, PARTS)),
-            dma((ns, 4)),
-            dma((ns, 4)),
-            dma((2,)),
-            dma((2,)),
+            dma((ns, 3)),
+            dma((ns, 3)),
+            dma((2, ns - 1)),
+            dma((2, ns - 1)),
             dma,
             dma,
             dma((2, nf - 1)),
             dma((2, nf - 1)),
             dma((ns,)),
             dma((ns,)),
+            dma((2,)),
+            dma((2,)),
+            dma((2,)),
+            dma((2,)),
+            dma((nf,)),
+            dma((nf,)),
+            dma((nf,)),
+            dma((nf,)),
         ],
         compiler_params=pltpu.CompilerParams(
             collective_id=0, has_side_effects=True, vmem_limit_bytes=54 * 1024 * 1024
@@ -801,7 +930,7 @@
     heads_here = MEMORY_HEADS // (lax.axis_size("fs") * lax.axis_size("tp"))
     channels = w_conv_gate.shape[1]
     ns, nf, nt = (lax.axis_size("sp"), lax.axis_size("fs"), lax.axis_size("tp"))
-    if 2 <= ns <= 8 and nf == 4 and nt == 2 and heads_here == 1 and channels == HEAD_DIM:
+    if ns == 4 and nf == 4 and nt == 2 and heads_here == 1 and channels == HEAD_DIM:
         return whole_layer(
             activations[0],
             norm_gain[None, :],

time: 86.3 us -> 81.5 us (0.944)
  the two profiles are of different devices: /device:TPU:25 before, /device:TPU:0 now
where the time goes in v3:
time: 81.5 us; the launch traced here: 81.4 us
  Pallas kernels  80.6 us (99%)
    pallas_call x1, Pallas kernels, whole_layer(): pl.pallas_call(functools.partial(layer_kernel, ns, nf), out_shape=pltpu.V...  80.6 us

profile of v3, /device:TPU:0, one launch (start us, length us, event | category | flops | bytes accessed | tf_op | source)
XLA Modules:
  0.0 81.4 jit_solution(11308769858874585347)
XLA Ops:
  0.0 80.6 %shard_map.154 = bf16[128,2048]{1,0:T(8,128)(2,1)S(1)} custom-call(bf16[256,2048]{1,0:T(8,128)(2,1)} %bitcast.8, f32[1,2048]{1,0:T(1,128)} %bitcast.12, bf16[512,128]{1,0:T(8,128)(2,1)} %w0_ref.1, bf16[512,128]{1,0:T(8,128)(2,1)} %w1_ref.1, bf16[512,128]{1,0:T(8,128)(2,1)} %w2_ref.1, bf16[512,128]{1,0:T(8,128)(2,1)} %w3_ref.1, bf16[512,128]{1,0:T(8,128)(2,1)} %w4_ref.1, ...), custom_call_target="tpu_custom_call" | custom-call | tf_op jit(solution)/shard_map/pallas_call | solution.py:843
  80.6 0.8 copy.18

commit v4 on v3

--- a/solution.py
+++ b/solution.py
@@ -190,6 +190,7 @@
     guest_padded,
     guest_mine,
     acc,
+    share,
     other,
     load_sem,
     x_send,
@@ -273,10 +274,15 @@
     for peer in beside:
         pl.semaphore_signal(barrier, inc=1, device_id=(sp, peer, tp), device_id_type=MESH)
         pl.semaphore_signal(barrier, inc=1, device_id=(pair, peer, tp), device_id_type=MESH)
-    for off in range(1, ns):
-        there = (lax.rem(sp + off, ns), fs, tp)
-        pl.semaphore_signal(barrier, inc=1, device_id=there, device_id_type=MESH)
     pl.semaphore_signal(barrier, inc=1, device_id=partner, device_id_type=MESH)
+
+    @pl.when(has_up)
+    def _():
+        pl.semaphore_signal(barrier, inc=1, device_id=up, device_id_type=MESH)
+
+    @pl.when(has_down)
+    def _():
+        pl.semaphore_signal(barrier, inc=1, device_id=down, device_id_type=MESH)
 
     def place(part, owner):
         if part == OUT:
@@ -323,23 +329,53 @@
             there,
             p_send.at[owner, way],
             p_recv.at[owner, way],
-            (sp, beside[(0, 1, 0)[way]], tp),
+            (sp, beside[(0, 1, 0, 1)[way]], tp),
         )
 
     def spread(owner):
         for way in range(2):
             p_copy(owner, way, fs).start()
 
-    def pass_on(owner):
-        p_copy(owner, 1, beside[1]).wait_recv()
-        p_copy(owner, 2, beside[1]).start()
-
-    def pass_step(d):
+    def side_of(d):
+        return 1 if 0 < d < ns - 1 else 0
+
+    def each_block(d, use):
+        if d == 0:
+            use(sp)
+            return
         for side in range(2):
 
             @pl.when(arrives(OUT, side, d))
             def _():
-                pass_on(owner_of(side, d))
+                use(owner_of(side, d))
+
+    def pass_step(d):
+        side = side_of(d)
+
+        def use(owner):
+            p_copy(owner, side, beside[side]).wait_recv()
+            p_copy(owner, 3 - side, beside[side]).start()
+
+        each_block(d, use)
+
+    def rest_step(d):
+        side = side_of(d)
+
+        def use(owner):
+            p_copy(owner, 1 - side, beside[1 - side]).wait_recv()
+            p_copy(owner, 3 - side, beside[2]).wait_recv()
+
+        each_block(d, use)
+
+    def drain_step(d):
+        side = side_of(d)
+
+        def use(owner):
+            for way in range(2):
+                p_copy(owner, way, fs).wait_send()
+            p_copy(owner, 3 - side, beside[side]).wait_send()
+
+        each_block(d, use)
 
     def z_step(part, d):
         for side in range(2):
@@ -376,9 +412,9 @@
             (pair, fs, tp),
         )
 
-    def u_copy(j, seq):
+    def u_copy(seq):
         there = guest_rows(guest, seq, tp)
-        return remote(there, there, u_send.at[j], u_recv.at[j], (sp, beside[1], tp))
+        return remote(there, there, u_send, u_recv, (sp, beside[1], tp))
 
     def v_copy(k, part):
         there = guest_rows(guest, around[k], part)
@@ -388,14 +424,15 @@
         @pl.when(hosts)
         def _():
             t_copy(j).wait_recv()
-            u_copy(j, around[j]).start()
+            if j == 1:
+                u_copy(around[1]).start()
             v_copy(j, tp).start()
 
-    def guest_from_beside(j):
+    def guest_from_beside():
         @pl.when(hosts)
         def _():
-            u_copy(j, around[2 + j]).wait_recv()
-            v_copy(2 + j, tp).start()
+            u_copy(around[3]).wait_recv()
+            v_copy(3, tp).start()
 
     def guest_to_pair(j):
         @pl.when(guests)
@@ -437,31 +474,28 @@
             mix_copy(m, k, beside[k], fs).start()
         got[m, :, block(fs, cols)] = mine[m, fs]
 
-    def state_copies(off, source):
-        to = (lax.rem(sp + off, ns), fs, tp)
+    def state_copies(d, source):
+        here = (local_stat, passed) if d == 0 else (stats.at[source], states.at[source])
         return (
-            remote(
-                local_stat, stats.at[source], s_send.at[0, off - 1], s_recv.at[0, off - 1], to
-            ),
-            remote(passed, states.at[source], s_send.at[1, off - 1], s_recv.at[1, off - 1], to),
-        )
-
-    def states_out():
-        for off in range(ns - 1, 0, -1):
-
-            @pl.when(sp + off < ns)
-            def _():
-                for copy in state_copies(off, sp):
-                    copy.start()
-
-    def states_in():
-        for off in range(1, ns):
-
-            @pl.when(sp - off >= 0)
-            def _():
-                for copy in state_copies(off, sp - off):
-                    copy.wait_recv()
-
+            remote(here[0], stats.at[source], s_send.at[0, d], s_recv.at[0, d], up),
+            remote(here[1], states.at[source], s_send.at[1, d], s_recv.at[1, d], up),
+        )
+
+    def state_send(d):
+        @pl.when(has_up & (sp - d >= 0))
+        def _():
+            for copy in state_copies(d, sp - d):
+                copy.start()
+
+    def state_step(d):
+        @pl.when(sp - d >= 0)
+        def _():
+            for copy in state_copies(d - 1, sp - d):
+                copy.wait_recv()
+            if d < ns - 1:
+                state_send(d)
+
+    def join_states():
         carry[...] = jnp.zeros_like(carry)
         carry_m[...] = jnp.zeros_like(carry_m)
         for source in range(ns - 1):
@@ -545,12 +579,10 @@
 
     loads[2].wait()
     loads[3].wait()
-    pl.semaphore_wait(barrier, 2 * (nf - 1) + ns)
+    pl.semaphore_wait(
+        barrier, 2 * nf - 1 + has_up.astype(jnp.int32) + has_down.astype(jnp.int32)
+    )
     own(KV)
-    loads[8].wait()
-    loads[9].wait()
-    own(OUT)
-    spread(sp)
     loads[0].wait()
     loads[1].wait()
     step = 32
@@ -563,35 +595,31 @@
         return carried
 
     lax.fori_loop(0, half // step, norm_rows, 0)
-    loads[4].wait()
-    own(QUERY)
-    for j in (5, 6, 7):
-        loads[j].wait()
-    own(GATE)
     for way in range(2):
         x_copy(way, fs).start()
     d_copy(0, fs, tp).start()
-    z_step(OUT, 1)
+    loads[8].wait()
+    loads[9].wait()
+    own(OUT)
     z_step(KV, 1)
-    guest_to_pair(0)
+    spread(sp)
+    loads[5].wait()
+    loads[6].wait()
+    own(MIX)
     for way in range(2):
         activations_in(way)
-    pass_on(sp)
-    z_step(QUERY, 1)
-    z_step(OUT, 2)
-    own(MIX)
+    guest_to_pair(1)
+    z_step(OUT, 1)
     z_step(KV, 2)
-    z_step(QUERY, 2)
-    guest_to_pair(1)
-    pass_step(1)
-    z_step(MIX, 1)
     for way in range(2, 4):
         x_copy(way, beside[2]).wait_recv()
     d_copy(3, beside[2], tp).start()
-    z_step(OUT, 3)
+    loads[7].wait()
+    own(GATE)
+    loads[4].wait()
+    own(QUERY)
+    z_step(OUT, 2)
     z_step(KV, 3)
-    z_step(GATE, 1)
-    guest_from_pair(0)
     for j in range(10, 16):
         loads[j].wait()
     for k, seq in enumerate(around):
@@ -641,24 +669,25 @@
         local_stat[s : s + 1, :] = jnp.broadcast_to(total, (1, 128))
         local_stat[nf + s : nf + s + 1, :] = jnp.broadcast_to(peak, (1, 128))
 
+    guest_from_pair(1)
+    state_send(0)
+    guest_to_pair(2)
+    z_step(QUERY, 1)
+    z_step(OUT, 3)
+    pass_step(0)
+    guest_to_pair(0)
+    state_step(1)
+    z_step(MIX, 1)
+    z_step(GATE, 1)
+    pass_step(1)
+    state_step(2)
+    z_step(QUERY, 2)
+    state_step(3)
+    pass_step(2)
+    pass_step(3)
     z_step(QUERY, 3)
-    z_step(GATE, 2)
-    states_out()
-    pass_step(2)
-    guest_from_pair(1)
-    pass_step(3)
-    guest_from_beside(0)
-    z_step(MIX, 2)
-    own_products()
-
-    @pl.when(hosts)
-    def _():
-        for k in range(nf - 1):
-            guest_part(k)
-            if k > 0:
-                c_copy(k - 1, around[k - 1], fs).start()
-
-    states_in()
+    guest_from_pair(2)
+    join_states()
     project(QUERY, query)
 
     scale = HEAD_DIM ** (-0.5)
@@ -687,6 +716,10 @@
         mine[1, s] = (cell * head_gain).astype(BF16)
 
     hand_out(1)
+    z_step(MIX, 2)
+    z_step(GATE, 2)
+    guest_from_beside()
+    own_products()
 
     @pl.when(outer)
     def _():
@@ -694,28 +727,29 @@
 
     @pl.when(hosts)
     def _():
-        c_copy(nf - 2, around[nf - 2], fs).start()
+        guest_part(1)
         mine[0, beside[0]] = own_part(beside[0])
+        c_copy(1, around[1], fs).start()
+        guest_part(3)
+        mix_copy(0, 0, beside[0], fs).start()
+        mine[0, beside[2]] = own_part(beside[2])
+        c_copy(3, around[3], fs).start()
+        guest_part(2)
+        mix_copy(0, 2, beside[2], fs).start()
         mine[0, beside[1]] = own_part(beside[1])
-        mix_copy(0, 0, beside[0], fs).start()
-        got[0, :, block(fs, cols)] = own_part(fs)
-        mix_copy(0, 1, beside[1], fs).start()
-
-    guest_from_beside(1)
+        c_copy(2, around[2], fs).start()
+
+    guest_from_pair(0)
 
     @pl.when(hosts)
     def _():
-        guest_part(nf - 1)
-        mine[0, beside[2]] = own_part(beside[2])
-        c_copy(nf - 1, around[nf - 1], fs).start()
-        mix_copy(0, 2, beside[2], fs).start()
-
-    def arrived(owner, carried):
-        p_copy(owner, 0, beside[0]).wait_recv()
-        p_copy(owner, 2, beside[2]).wait_recv()
-        return carried
-
-    lax.fori_loop(0, ns, arrived, 0)
+        guest_part(0)
+        mix_copy(0, 1, beside[1], fs).start()
+        got[0, :, block(fs, cols)] = own_part(fs)
+        c_copy(0, around[0], fs).start()
+
+    for d in range(ns):
+        rest_step(d)
     for k in range(nf - 1):
         mix_copy(1, k, beside[k], beside[k]).wait_recv()
 
@@ -729,7 +763,7 @@
 
     def e_copy(i):
         return remote(
-            acc.at[block(1 - tp, half), block(i, ocols)],
+            share.at[:, block(i, ocols)],
             other.at[:, block(i, ocols)],
             e_send.at[i],
             e_recv.at[i],
@@ -743,50 +777,40 @@
             preferred_element_type=F32,
         )
 
-    @pl.when(hosts)
-    def _():
-        mix_copy(0, 0, beside[0], beside[0]).wait_recv()
-
-    @pl.when(guests)
-    def _():
-        for k in range(2):
-            c_copy(k, around[k], around[k]).wait_recv()
-
+    def conv_in(hosted, guested):
+        @pl.when(hosts)
+        def _():
+            for k in hosted:
+                mix_copy(0, k, beside[k], beside[k]).wait_recv()
+
+        @pl.when(guests)
+        def _():
+            for k in guested:
+                c_copy(k, around[k], around[k]).wait_recv()
+
+    conv_in((1, 2), (2, 3))
+    for i in range(ns):
+        add_pair(i, 1 - fy)
+    conv_in((0,), (0, 1))
     for i in range(ns):
         add_pair(i, fy)
-
-    @pl.when(hosts)
-    def _():
-        for k in (1, 2):
-            mix_copy(0, k, beside[k], beside[k]).wait_recv()
-
-    @pl.when(guests)
-    def _():
-        for k in range(2, nf):
-            c_copy(k, around[k], around[k]).wait_recv()
-
-    for i in range(ns):
-        add_pair(i, 1 - fy)
+        share[:, block(i, ocols)] = acc[block(1 - tp, half), block(i, ocols)].astype(BF16)
         if i > 0:
             e_copy(i - 1).start()
     e_copy(ns - 1).start()
-
-    def merge(i, carried):
+    for i in range(ns):
         e_copy(i).wait_recv()
         out_ref[:, block(i, ocols)] = (
-            acc[block(tp, half), block(i, ocols)] + other[:, block(i, ocols)]
+            acc[block(tp, half), block(i, ocols)] + other[:, block(i, ocols)].astype(F32)
         ).astype(BF16)
-        return carried
-
-    lax.fori_loop(0, ns, merge, 0)
 
     def sent(i, carried):
         e_copy(i).wait_send()
-        for way in range(3):
-            p_copy(i, way, (fs, fs, beside[1])[way]).wait_send()
         return carried
 
     lax.fori_loop(0, ns, sent, 0)
+    for d in range(ns):
+        drain_step(d)
     for way in range(4):
         x_copy(way, (fs, fs, beside[0], beside[1])[way]).wait_send()
     for k, seq in enumerate(around):
@@ -801,12 +825,11 @@
         for k in range(nf):
             v_copy(k, tp).wait_send()
             c_copy(k, around[k], fs).wait_send()
-        for j in range(2):
-            u_copy(j, around[j]).wait_send()
+        u_copy(around[1]).wait_send()
 
     @pl.when(guests)
     def _():
-        for j in range(2):
+        for j in range(nf - 1):
             t_copy(j).wait_send()
 
     @pl.when(inner)
@@ -822,11 +845,11 @@
                     for part in parts:
                         z_copy(part, side, d, owner_of(side, d)).wait_send()
 
-    for off in range(1, ns):
-
-        @pl.when(sp + off < ns)
-        def _():
-            for copy in state_copies(off, sp):
+    for d in range(ns - 1):
+
+        @pl.when(has_up & (sp - d >= 0))
+        def _():
+            for copy in state_copies(d, sp - d):
                 copy.wait_send()
 
 
@@ -875,7 +898,8 @@
             vmem((nf, RIM + tokens, cols), F32),
             vmem((nf, tokens, cols), BF16),
             vmem((tokens, ns * ocols), F32),
-            vmem((half, ns * ocols), F32),
+            vmem((half, ns * ocols), BF16),
+            vmem((half, ns * ocols), BF16),
             dma((16,)),
             dma((4,)),
             dma((4,)),
@@ -883,8 +907,8 @@
             dma((nf,)),
             dma((2, ns - 1, PARTS)),
             dma((2, ns - 1, PARTS)),
-            dma((ns, 3)),
-            dma((ns, 3)),
+            dma((ns, 4)),
+            dma((ns, 4)),
             dma((2, ns - 1)),
             dma((2, ns - 1)),
             dma,
@@ -893,10 +917,10 @@
             dma((2, nf - 1)),
             dma((ns,)),
             dma((ns,)),
-            dma((2,)),
-            dma((2,)),
-            dma((2,)),
-            dma((2,)),
+            dma((nf - 1,)),
+            dma((nf - 1,)),
+            dma,
+            dma,
             dma((nf,)),
             dma((nf,)),
             dma((nf,)),

time: 81.5 us -> 75.8 us (0.930)
  the two profiles are of different devices: /device:TPU:0 before, /device:TPU:25 now
where the time goes in v4:
time: 75.8 us; the launch traced here: 74.7 us
  Pallas kernels  73.9 us (97%)
  local copies, waits for them, and re-layouts  0.8 us (1%)
    pallas_call x1, Pallas kernels, whole_layer(): pl.pallas_call(functools.partial(layer_kernel, ns, nf), out_shape=pltpu.V...  73.9 us

profile of v4, /device:TPU:25, one launch (start us, length us, event | category | flops | bytes accessed | tf_op | source)
XLA Modules:
  0.0 74.7 jit_solution(15784606583199971445)
XLA Ops:
  0.0 73.9 %shard_map.154 = bf16[128,2048]{1,0:T(8,128)(2,1)S(1)} custom-call(bf16[256,2048]{1,0:T(8,128)(2,1)} %bitcast.8, f32[1,2048]{1,0:T(1,128)} %bitcast.12, bf16[512,128]{1,0:T(8,128)(2,1)} %w0_ref.1, bf16[512,128]{1,0:T(8,128)(2,1)} %w1_ref.1, bf16[512,128]{1,0:T(8,128)(2,1)} %w2_ref.1, bf16[512,128]{1,0:T(8,128)(2,1)} %w3_ref.1, bf16[512,128]{1,0:T(8,128)(2,1)} %w4_ref.1, ...), custom_call_target="tpu_custom_call" | custom-call | tf_op jit(solution)/shard_map/pallas_call | solution.py:866
  73.9 0.8 %copy.18 = bf16[1,128,2048]{2,1,0:T(8,128)(2,1)} copy(bf16[1,128,2048]{2,1,0:T(8,128)(2,1)S(1)} %bitcast.7) | data formatting | bytes 1048576

commit v5 on v4

--- a/solution.py
+++ b/solution.py
@@ -189,6 +189,8 @@
     guest,
     guest_padded,
     guest_mine,
+    last,
+    wo_last,
     acc,
     share,
     other,
@@ -217,6 +219,8 @@
     v_recv,
     c_send,
     c_recv,
+    l_send,
+    l_recv,
 ):
     sp, fs, tp = (lax.axis_index("sp"), lax.axis_index("fs"), lax.axis_index("tp"))
     g = fs * 2 + tp
@@ -267,14 +271,15 @@
     )
     for j, (ref, held) in enumerate(smalls):
         loads.append(pltpu.make_async_copy(ref, held, load_sem.at[10 + j]))
-    for j in (2, 3, 0, 1, 4, 8, 9, 5, 6, 7, 10, 11, 12, 13, 14, 15):
+    for j in (0, 1, 2, 3, 8, 9, 5, 6, 7, 4, 10, 11, 12, 13, 14, 15):
         loads[j].start()
 
     barrier = pltpu.get_barrier_semaphore()
     for peer in beside:
         pl.semaphore_signal(barrier, inc=1, device_id=(sp, peer, tp), device_id_type=MESH)
         pl.semaphore_signal(barrier, inc=1, device_id=(pair, peer, tp), device_id_type=MESH)
-    pl.semaphore_signal(barrier, inc=1, device_id=partner, device_id_type=MESH)
+    for there in (partner, (pair, fs, 1 - tp)):
+        pl.semaphore_signal(barrier, inc=1, device_id=there, device_id_type=MESH)
 
     @pl.when(has_up)
     def _():
@@ -403,10 +408,18 @@
     def guest_rows(ref, seq, part):
         return ref.at[pl.ds(pl.multiple_of(seq * tokens + part * half, half), half)]
 
+    quarter = half // 2
+
+    def piece(ref, j, part):
+        if j in (0, nf - 1):
+            first = fs * tokens + part * half + (0 if j == 0 else quarter)
+            return ref.at[pl.ds(pl.multiple_of(first, quarter), quarter)]
+        return guest_rows(ref, around[j], part)
+
     def t_copy(j):
         return remote(
-            guest_rows(normed, around[j], tp),
-            guest_rows(guest, around[j], tp),
+            piece(normed, j, tp),
+            piece(guest, j, tp),
             t_send.at[j],
             t_recv.at[j],
             (pair, fs, tp),
@@ -419,6 +432,11 @@
     def v_copy(k, part):
         there = guest_rows(guest, around[k], part)
         return remote(there, there, v_send.at[k], v_recv.at[k], partner)
+
+    def v_piece(j, part):
+        at = 0 if j == 0 else nf
+        there = piece(guest, j, part)
+        return remote(there, there, v_send.at[at], v_recv.at[at], partner)
 
     def guest_from_pair(j):
         @pl.when(hosts)
@@ -426,7 +444,10 @@
             t_copy(j).wait_recv()
             if j == 1:
                 u_copy(around[1]).start()
-            v_copy(j, tp).start()
+            if j in (0, nf - 1):
+                v_piece(j, tp).start()
+            else:
+                v_copy(j, tp).start()
 
     def guest_from_beside():
         @pl.when(hosts)
@@ -550,6 +571,19 @@
             (pair, around[k], tp),
         )
 
+    def last_copy(k, source):
+        core = tp if k == 0 else 1 - tp
+        return remote(
+            guest_mine.at[fs, block(core, half)],
+            last.at[:, block(source, cols)],
+            c_send.at[k],
+            c_recv.at[k],
+            (pair, fs, core),
+        )
+
+    def row_copy():
+        return remote(wo.at[0, block(fs, cols)], wo_last, l_send, l_recv, partner)
+
     def own_products():
         @pl.when(hosts)
         def _():
@@ -565,7 +599,11 @@
 
     def guest_part(k):
         seq = around[k]
-        v_copy(k, 1 - tp).wait_recv()
+        if k == 0:
+            v_piece(0, 1 - tp).wait_recv()
+            v_piece(nf - 1, 1 - tp).wait_recv()
+        else:
+            v_copy(k, 1 - tp).wait_recv()
         gate = products(guest, seq, guest_padded)
         guest_padded[seq, 0:RIM, :] = jnp.where(inner, 0.0, padded[seq, tokens : tokens + RIM, :])
         guest_mine[seq] = convolve(guest_padded, seq, gate)
@@ -577,12 +615,6 @@
 
         return convolve(padded, seq, gated[tile(seq), :])
 
-    loads[2].wait()
-    loads[3].wait()
-    pl.semaphore_wait(
-        barrier, 2 * nf - 1 + has_up.astype(jnp.int32) + has_down.astype(jnp.int32)
-    )
-    own(KV)
     loads[0].wait()
     loads[1].wait()
     step = 32
@@ -595,6 +627,12 @@
         return carried
 
     lax.fori_loop(0, half // step, norm_rows, 0)
+    loads[2].wait()
+    loads[3].wait()
+    pl.semaphore_wait(
+        barrier, 2 * nf + has_up.astype(jnp.int32) + has_down.astype(jnp.int32)
+    )
+    own(KV)
     for way in range(2):
         x_copy(way, fs).start()
     d_copy(0, fs, tp).start()
@@ -619,7 +657,6 @@
     loads[4].wait()
     own(QUERY)
     z_step(OUT, 2)
-    z_step(KV, 3)
     for j in range(10, 16):
         loads[j].wait()
     for k, seq in enumerate(around):
@@ -656,6 +693,7 @@
     sums = jnp.where(line < nf, sums, packed)
     logs_t[...] = sums
     logs[...] = sums.T
+    z_step(KV, 3)
     project(KV, kv)
     for s in range(nf):
         rows = pl.ds(s * tokens, tokens)
@@ -674,8 +712,14 @@
     guest_to_pair(2)
     z_step(QUERY, 1)
     z_step(OUT, 3)
+
+    @pl.when(guests)
+    def _():
+        row_copy().start()
+
     pass_step(0)
     guest_to_pair(0)
+    guest_to_pair(nf - 1)
     state_step(1)
     z_step(MIX, 1)
     z_step(GATE, 1)
@@ -738,15 +782,17 @@
         mix_copy(0, 2, beside[2], fs).start()
         mine[0, beside[1]] = own_part(beside[1])
         c_copy(2, around[2], fs).start()
+        mix_copy(0, 1, beside[1], fs).start()
 
     guest_from_pair(0)
+    guest_from_pair(nf - 1)
 
     @pl.when(hosts)
     def _():
         guest_part(0)
-        mix_copy(0, 1, beside[1], fs).start()
         got[0, :, block(fs, cols)] = own_part(fs)
-        c_copy(0, around[0], fs).start()
+        for k in (0, nf):
+            last_copy(k, tp).start()
 
     for d in range(ns):
         rest_step(d)
@@ -770,39 +816,71 @@
             partner,
         )
 
-    def add_pair(i, pair):
+    def add_conv(i, first, count):
         acc[:, block(i, ocols)] = acc[:, block(i, ocols)] + jnp.dot(
-            got[0, :, block(pair, 2 * cols)],
-            wo[0, block(pair, 2 * cols), block(i, ocols)],
+            got[0, :, pl.ds(first, count)],
+            wo[0, pl.ds(first, count), block(i, ocols)],
             preferred_element_type=F32,
         )
 
-    def conv_in(hosted, guested):
-        @pl.when(hosts)
-        def _():
-            for k in hosted:
-                mix_copy(0, k, beside[k], beside[k]).wait_recv()
-
-        @pl.when(guests)
-        def _():
-            for k in guested:
-                c_copy(k, around[k], around[k]).wait_recv()
-
-    conv_in((1, 2), (2, 3))
-    for i in range(ns):
-        add_pair(i, 1 - fy)
-    conv_in((0,), (0, 1))
-    for i in range(ns):
-        add_pair(i, fy)
+    def add_pair(i, pair_at):
+        add_conv(i, pl.multiple_of(pair_at * 2 * cols, 2 * cols), 2 * cols)
+
+    def hand_over(i):
         share[:, block(i, ocols)] = acc[block(1 - tp, half), block(i, ocols)].astype(BF16)
         if i > 0:
             e_copy(i - 1).start()
-    e_copy(ns - 1).start()
-    for i in range(ns):
-        e_copy(i).wait_recv()
-        out_ref[:, block(i, ocols)] = (
-            acc[block(tp, half), block(i, ocols)] + other[:, block(i, ocols)].astype(F32)
-        ).astype(BF16)
+        if i == ns - 1:
+            e_copy(i).start()
+
+    @pl.when(hosts)
+    def _():
+        for k in (1, 2):
+            mix_copy(0, k, beside[k], beside[k]).wait_recv()
+        for i in range(ns):
+            add_pair(i, 1 - fy)
+        mix_copy(0, 0, beside[0], beside[0]).wait_recv()
+        for i in range(ns):
+            add_pair(i, fy)
+            hand_over(i)
+        for i in range(ns):
+            e_copy(i).wait_recv()
+            out_ref[:, block(i, ocols)] = (
+                acc[block(tp, half), block(i, ocols)] + other[:, block(i, ocols)].astype(F32)
+            ).astype(BF16)
+
+    @pl.when(guests)
+    def _():
+        c_copy(1, around[1], around[1]).wait_recv()
+        for i in range(ns):
+            add_conv(i, pl.multiple_of(beside[0] * cols, cols), cols)
+        for k in range(2, nf):
+            c_copy(k, around[k], around[k]).wait_recv()
+        for i in range(ns):
+            add_pair(i, 1 - fy)
+            hand_over(i)
+        row_copy().wait_recv()
+        for i in range(ns):
+            e_copy(i).wait_recv()
+            acc[block(tp, half), block(i, ocols)] = acc[
+                block(tp, half), block(i, ocols)
+            ] + other[:, block(i, ocols)].astype(F32)
+        for k in (0, nf):
+            last_copy(k, tp if k == 0 else 1 - tp).wait_recv()
+        for i in range(ns):
+            out_ref[:, block(i, ocols)] = (
+                acc[block(tp, half), block(i, ocols)]
+                + jnp.dot(
+                    last[:, block(tp, cols)],
+                    wo[0, block(fs, cols), block(i, ocols)],
+                    preferred_element_type=F32,
+                )
+                + jnp.dot(
+                    last[:, block(1 - tp, cols)],
+                    wo_last[:, block(i, ocols)],
+                    preferred_element_type=F32,
+                )
+            ).astype(BF16)
 
     def sent(i, carried):
         e_copy(i).wait_send()
@@ -822,15 +900,21 @@
     def _():
         for k in range(nf - 1):
             mix_copy(0, k, beside[k], fs).wait_send()
-        for k in range(nf):
+        for k in range(1, nf):
             v_copy(k, tp).wait_send()
+        for j in (0, nf - 1):
+            v_piece(j, tp).wait_send()
+        for k in range(1, nf):
             c_copy(k, around[k], fs).wait_send()
+        for k in (0, nf):
+            last_copy(k, tp).wait_send()
         u_copy(around[1]).wait_send()
 
     @pl.when(guests)
     def _():
-        for j in range(nf - 1):
+        for j in range(nf):
             t_copy(j).wait_send()
+        row_copy().wait_send()
 
     @pl.when(inner)
     def _():
@@ -897,6 +981,8 @@
             vmem((count, model), BF16),
             vmem((nf, RIM + tokens, cols), F32),
             vmem((nf, tokens, cols), BF16),
+            vmem((half, 2 * cols), BF16),
+            vmem((cols, ns * ocols), BF16),
             vmem((tokens, ns * ocols), F32),
             vmem((half, ns * ocols), BF16),
             vmem((half, ns * ocols), BF16),
@@ -917,14 +1003,16 @@
             dma((2, nf - 1)),
             dma((ns,)),
             dma((ns,)),
-            dma((nf - 1,)),
-            dma((nf - 1,)),
+            dma((nf,)),
+            dma((nf,)),
             dma,
             dma,
-            dma((nf,)),
-            dma((nf,)),
-            dma((nf,)),
-            dma((nf,)),
+            dma((nf + 1,)),
+            dma((nf + 1,)),
+            dma((nf + 1,)),
+            dma((nf + 1,)),
+            dma,
+            dma,
         ],
         compiler_params=pltpu.CompilerParams(
             collective_id=0, has_side_effects=True, vmem_limit_bytes=54 * 1024 * 1024

time: 75.8 us -> 73.7 us (0.972)
  Pallas kernels: 73.9 us -> 72.2 us
    pallas_call x1, Pallas kernels: 73.9 us -> 72.2 us  [whole_layer(): pl.pallas_call(functools.partial(layer_kernel, ns, nf), out_shape=pltpu.V...]
where the time goes in v5:
time: 73.7 us; the launch traced here: 73 us
  Pallas kernels  72.2 us (98%)
  local copies, waits for them, and re-layouts  0.8 us (1%)
    pallas_call x1, Pallas kernels, whole_layer(): pl.pallas_call(functools.partial(layer_kernel, ns, nf), out_shape=pltpu.V...  72.2 us

profile of v5, /device:TPU:25, one launch (start us, length us, event | category | flops | bytes accessed | tf_op | source)
XLA Modules:
  0.0 73.0 jit_solution(11441152444220219423)
XLA Ops:
  0.0 72.2 %shard_map.154 = bf16[128,2048]{1,0:T(8,128)(2,1)S(1)} custom-call(bf16[256,2048]{1,0:T(8,128)(2,1)} %bitcast.8, f32[1,2048]{1,0:T(1,128)} %bitcast.12, bf16[512,128]{1,0:T(8,128)(2,1)} %w0_ref.1, bf16[512,128]{1,0:T(8,128)(2,1)} %w1_ref.1, bf16[512,128]{1,0:T(8,128)(2,1)} %w2_ref.1, bf16[512,128]{1,0:T(8,128)(2,1)} %w3_ref.1, bf16[512,128]{1,0:T(8,128)(2,1)} %w4_ref.1, ...), custom_call_target="tpu_custom_call" | custom-call | tf_op jit(solution)/shard_map/pallas_call | solution.py:950
  72.2 0.8 %copy.18 = bf16[1,128,2048]{2,1,0:T(8,128)(2,1)} copy(bf16[1,128,2048]{2,1,0:T(8,128)(2,1)S(1)} %bitcast.7) | data formatting | bytes 1048576

commit v6 on v5

--- a/solution.py
+++ b/solution.py
@@ -726,13 +726,12 @@
     pass_step(1)
     state_step(2)
     z_step(QUERY, 2)
-    state_step(3)
     pass_step(2)
     pass_step(3)
     z_step(QUERY, 3)
-    guest_from_pair(2)
+    project(QUERY, query)
+    state_step(3)
     join_states()
-    project(QUERY, query)
 
     scale = HEAD_DIM ** (-0.5)
     head_gain = head[:, block(g, cols)]
@@ -760,6 +759,7 @@
         mine[1, s] = (cell * head_gain).astype(BF16)
 
     hand_out(1)
+    guest_from_pair(2)
     z_step(MIX, 2)
     z_step(GATE, 2)
     guest_from_beside()

time: 73.7 us -> 73.6 us (level)
  the two profiles are of different devices: /device:TPU:25 before, /device:TPU:0 now
where the time goes in v6:
time: 73.6 us; the launch traced here: 73.5 us
  Pallas kernels  72.6 us (99%)
  local copies, waits for them, and re-layouts  0.8 us (1%)
    pallas_call x1, Pallas kernels, whole_layer(): pl.pallas_call(functools.partial(layer_kernel, ns, nf), out_shape=pltpu.V...  72.6 us

profile of v6, /device:TPU:0, one launch (start us, length us, event | category | flops | bytes accessed | tf_op | source)
XLA Modules:
  0.0 73.5 jit_solution(10068338583319243860)
XLA Ops:
  0.0 72.6 %shard_map.154 = bf16[128,2048]{1,0:T(8,128)(2,1)S(1)} custom-call(bf16[256,2048]{1,0:T(8,128)(2,1)} %bitcast.8, f32[1,2048]{1,0:T(1,128)} %bitcast.12, bf16[512,128]{1,0:T(8,128)(2,1)} %w0_ref.1, bf16[512,128]{1,0:T(8,128)(2,1)} %w1_ref.1, bf16[512,128]{1,0:T(8,128)(2,1)} %w2_ref.1, bf16[512,128]{1,0:T(8,128)(2,1)} %w3_ref.1, bf16[512,128]{1,0:T(8,128)(2,1)} %w4_ref.1, ...), custom_call_target="tpu_custom_call" | custom-call | tf_op jit(solution)/shard_map/pallas_call | solution.py:950
  72.7 0.8 %copy.18 = bf16[1,128,2048]{2,1,0:T(8,128)(2,1)} copy(bf16[1,128,2048]{2,1,0:T(8,128)(2,1)S(1)} %bitcast.7) | data formatting | bytes 1048576
